TPU v7x, 32 devices: a whole 2x2x4 slice. The times are simulated.
32 devices in a mesh: sp: 8 (over z, core), tp: 4 (over y, x).
Axes of the slice: x: 2, y: 2, z: 4, core: 2. Of those that a mesh axis runs over, the one named last changes fastest.
Arguments:
- residual_in: bfloat16 [2048, 2048], P('sp'), may hold values from -3 to 3
- mix_gain: float32 [2048], replicated, may hold values from 0.1 to 1.9
- pool_weight: bfloat16 [512, 2048], P(None, 'tp'), may hold values from -0.5 to 0.5
- pool_scale: float32 [2048], P('tp'), may hold values from 0.1 to 1.9
- ffn_gain: float32 [2048], replicated, may hold values from 0.1 to 1.9
- route_ids: int32 [2048, 2], P('sp'), may hold values from 0 to 7, all different within a row; in each aligned block of 64 rows (0 to 63, 64 to 127, ...) at most 32 rows name the same one
- route_weights: float32 [2048, 2], P('sp'), may hold values from 0.1 to 1
- gate_weight: bfloat16 [8, 2048, 3584], P('sp', None, 'tp'), may hold values from -0.125 to 0.125
- up_weight: bfloat16 [8, 2048, 3584], P('sp', None, 'tp'), may hold values from -0.125 to 0.125
- down_weight: bfloat16 [8, 3584, 2048], P('sp', 'tp'), may hold values from -0.09375 to 0.09375
Outputs:
- layer_out: bfloat16 [2048, 2048], P('sp')
Inputs may be any that keep to these rules, and one draw needn't show every extreme that they name: `route_ids`: each row names 2 different experts; in each aligned block of 64 rows no expert is named by more than 32 rows, and some block has an expert named by exactly 32 rows.
All inputs are finite; a program needn't handle non-finite values.
Results may differ from a plain program's by a relative error of at most 0.0074.
Values may be sent and summed in bfloat16 or wider, within the bound.
A program may use at most 64 MiB of HBM per device.

v0:
```python
import functools

import jax
import jax.numpy as jnp
from jax import lax
from jax.experimental import pallas as pl
from jax.experimental.pallas import tpu as pltpu
from jax.sharding import PartitionSpec as P

GROUPS = 4
SPAN = 16
TOP_K = 2
CORES = 2
SIDE = 2
EPS = 1e-06
MESH = pl.DeviceIdType.MESH
ZU, ZD, X, Y, DX, DY, FX, FY, FDX, FDY = range(10)

def from_behind(value, axis, steps):
    count = lax.axis_size(axis)
    first, last = (max(0, -steps), min(count, count - steps))
    return lax.ppermute(value, axis, [(source, source + steps) for source in range(first, last)])


def rms_scale(values, gain):
    return values * lax.rsqrt(jnp.mean(values * values, axis=-1, keepdims=True) + EPS) * gain


def slot_table(chosen_ids, experts, capacity):
    flat_ids = chosen_ids.reshape(-1)
    matches = (flat_ids[:, None] == jnp.arange(experts, dtype=jnp.int32)[None, :]).astype(jnp.int32)
    before = jnp.cumsum(matches, axis=0) - matches
    slot_of = jnp.sum(before * matches, axis=1)
    target = flat_ids * capacity + slot_of
    return (target[:, None] == jnp.arange(experts * capacity, dtype=jnp.int32)[None, :]).astype(
        jnp.float32
    )


def shards_any(
    residual_in,
    mix_gain,
    pool_weight,
    pool_scale,
    ffn_gain,
    route_ids,
    route_weights,
    gate_weight,
    up_weight,
    down_weight,
):
    tp_count = lax.axis_size("tp")
    sp_count = lax.axis_size("sp")
    tp_index = lax.axis_index("tp")
    tok_count, width = residual_in.shape
    group_width = width // GROUPS
    col_count = pool_weight.shape[1]
    row_count = tok_count // tp_count
    capacity = 2 * TOP_K * row_count // sp_count
    group_index = tp_index * col_count // group_width
    window = jnp.power(2, group_index + 1)
    stream = residual_in.astype(jnp.float32)
    inverse = lax.rsqrt(jnp.mean(stream * stream, axis=-1, keepdims=True) + EPS)
    stream_group = lax.dynamic_slice_in_dim(stream, group_index * group_width, group_width, 1)
    gain_group = lax.dynamic_slice_in_dim(mix_gain, group_index * group_width, group_width, 0)
    normed_group = (stream_group * inverse * gain_group).astype(jnp.bfloat16)
    rim_rows = from_behind(normed_group[tok_count - SPAN :], "sp", 1)
    extended = jnp.concatenate([rim_rows, normed_group], axis=0).astype(jnp.float32)
    window_sum = jnp.zeros((tok_count, group_width), jnp.float32)
    for offset in range(SPAN):
        window_sum = window_sum + jnp.where(
            offset < window, extended[SPAN - offset : SPAN - offset + tok_count], 0.0
        )
    position = lax.axis_index("sp") * tok_count + jnp.arange(tok_count, dtype=jnp.int32)
    divisor = jnp.minimum(position + 1, window).astype(jnp.float32)
    pooled = (window_sum / divisor[:, None] - extended[SPAN:]).astype(jnp.bfloat16)
    mixed = (jnp.dot(pooled, pool_weight, preferred_element_type=jnp.float32) * pool_scale).astype(
        jnp.bfloat16
    )
    stream_own = lax.dynamic_slice_in_dim(stream, tp_index * row_count, row_count, 0)
    mixed_own = lax.all_to_all(mixed, "tp", split_axis=0, concat_axis=1, tiled=True)
    after_own = (stream_own + mixed_own.astype(jnp.float32)).astype(jnp.bfloat16)
    normed_own = rms_scale(after_own.astype(jnp.float32), ffn_gain).astype(jnp.bfloat16)
    ids_own = lax.dynamic_slice_in_dim(route_ids, tp_index * row_count, row_count, 0)
    table_own = slot_table(ids_own, sp_count, capacity)
    repeated = jnp.repeat(normed_own, TOP_K, axis=0)
    outgoing = lax.dot_general(
        table_own.astype(jnp.bfloat16),
        repeated,
        (((0,), (0,)), ((), ())),
        preferred_element_type=jnp.float32,
    )
    outgoing = outgoing.astype(jnp.bfloat16).reshape(sp_count, capacity, width)
    arrived = lax.all_to_all(outgoing, "sp", split_axis=0, concat_axis=0, tiled=True)
    piece = lax.all_gather(arrived, "tp", axis=0, tiled=True)
    flat_rows = piece.reshape(-1, width)
    gate_part = jnp.dot(flat_rows, gate_weight[0], preferred_element_type=jnp.float32)
    up_part = jnp.dot(flat_rows, up_weight[0], preferred_element_type=jnp.float32)
    hidden = (jax.nn.silu(gate_part) * up_part).astype(jnp.bfloat16)
    hidden_all = hidden.reshape(piece.shape[0], piece.shape[1], hidden.shape[1])
    hidden_flat = hidden_all.reshape(-1, hidden_all.shape[-1])
    term = jnp.dot(hidden_flat, down_weight[0], preferred_element_type=jnp.float32)
    summed = lax.psum_scatter(
        term.astype(jnp.bfloat16).astype(jnp.float32).astype(jnp.bfloat16),
        "tp",
        scatter_dimension=0,
        tiled=True,
    )
    expert_out = summed.reshape(sp_count, capacity, width)
    returned_rows = lax.all_to_all(expert_out, "sp", split_axis=0, concat_axis=0, tiled=True)
    weights_own = lax.dynamic_slice_in_dim(route_weights, tp_index * row_count, row_count, 0)
    weight_table = jnp.einsum(
        "rk,rkc->rc", weights_own, table_own.reshape(row_count, TOP_K, sp_count * capacity)
    )
    expert_mix = jnp.dot(
        weight_table,
        returned_rows.reshape(-1, width).astype(jnp.float32),
        precision=lax.Precision.HIGHEST,
    )
    out_own = (after_own.astype(jnp.float32) + expert_mix).astype(jnp.bfloat16)
    return lax.all_gather(out_own, "tp", axis=0, tiled=True)


class Place:
    def __init__(self, send_sem, recv_sem):
        self.sp, self.tp = lax.axis_index("sp"), lax.axis_index("tp")
        self.levels = lax.axis_size("sp") // CORES
        self.z, self.c = self.sp // CORES, self.sp % CORES
        y, x = self.tp // SIDE, self.tp % SIDE
        self.tx = y * SIDE + (1 - x)
        self.ty = (1 - y) * SIDE + x
        self.td = (1 - y) * SIDE + (1 - x)
        self.send_sem, self.recv_sem = send_sem, recv_sem
        partner = self.z * CORES + (1 - self.c)
        self.partner = (partner, self.tp)
        self.to = {
            ZU: (self.sp + CORES, self.tp),
            ZD: (self.sp - CORES, self.tp),
            X: (self.sp, self.tx),
            Y: (self.sp, self.ty),
        }
        for kind, base in ((DX, X), (DY, Y), (FX, X), (FY, Y), (FDX, X), (FDY, Y)):
            self.to[kind] = self.to[base]

    def copy(self, kind, index, src, dst):
        return pltpu.make_async_remote_copy(
            src_ref=src,
            dst_ref=dst,
            send_sem=self.send_sem.at[kind, index],
            recv_sem=self.recv_sem.at[kind, index],
            device_id=self.to[kind],
            device_id_type=MESH,
        )

    def exists(self, offset):
        level = self.z + offset
        return (level >= 0) & (level < self.levels)

    def offsets(self):
        order = [0]
        for distance in range(1, self.levels):
            order += [-distance, distance]
        return order


def greet(place, everyone):
    barrier = pltpu.get_barrier_semaphore()

    def hello(target):
        pl.semaphore_signal(barrier, inc=1, device_id=target, device_id_type=MESH)

    hello(place.to[X])
    hello(place.to[Y])
    if everyone:
        count = lax.axis_size("sp")
        for step in range(1, count):
            hello((lax.rem(place.sp + step, count), place.tp))
        pl.semaphore_wait(barrier, count + 1)
    else:
        hello(place.partner)
        up, down = place.exists(1), place.exists(-1)
        pl.when(up)(lambda: hello(place.to[ZU]))
        pl.when(down)(lambda: hello(place.to[ZD]))
        pl.semaphore_wait(barrier, 3 + up.astype(jnp.int32) + down.astype(jnp.int32))


def gather_kernel(
    own_ref, meta_ref, result_ref, meta_out,
    out_ref, send_sem, recv_sem, p_send, p_recv, m_send, m_recv, l_sem, o_sem,
):
    place = Place(send_sem, recv_sem)
    rows, cols = own_ref.shape
    half = rows // 2
    z, c, tp = place.z, place.c, place.tp
    sp_count = lax.axis_size("sp")
    tiles = SIDE * SIDE

    def block(level, core, tile, first=0, count=rows):
        start = pl.multiple_of((level * CORES + core) * rows + first, half)
        return out_ref.at[pl.ds(start, count), pl.ds(pl.multiple_of(tile * cols, cols), cols)]

    def put_out(level, tile, core):
        start = pl.multiple_of((level * CORES + core) * rows, rows)
        lanes = pl.ds(pl.multiple_of(tile * cols, cols), cols)
        return pltpu.make_async_copy(
            block(level, core, tile),
            result_ref.at[pl.ds(start, rows), lanes],
            o_sem.at[level, tile, core],
        )

    def pair_copy(level, tile, core):
        ref = block(level, core, tile)
        return pltpu.make_async_remote_copy(
            src_ref=ref,
            dst_ref=ref,
            send_sem=p_send.at[level, tile],
            recv_sem=p_recv.at[level, tile],
            device_id=place.partner,
            device_id_type=MESH,
        )

    def meta_copy(step):
        target = lax.rem(place.sp + step, sp_count)
        return pltpu.make_async_remote_copy(
            src_ref=meta_ref,
            dst_ref=meta_out.at[place.sp],
            send_sem=m_send.at[step],
            recv_sem=m_recv.at[step],
            device_id=(target, tp),
            device_id_type=MESH,
        )

    local = pltpu.make_async_copy(own_ref, block(z, c, tp), l_sem.at[0])
    local.start()
    local_meta = pltpu.make_async_copy(meta_ref, meta_out.at[place.sp], l_sem.at[1])
    local_meta.start()
    local.wait()
    local_meta.wait()
    greet(place, True)

    def whole(kind, level, tile):
        ref = block(level, c, tile)
        return place.copy(kind, level, ref, ref)

    def part(kind, level, tile):
        ref = block(level, c, tile, 0 if kind == DY else half, half)
        return place.copy(kind, level, ref, ref)

    def first(offset):
        level = z + offset
        if offset < 0:
            whole(ZU, level, tp).wait_recv()
        if offset > 0:
            whole(ZD, level, tp).wait_recv()
        if offset <= 0:
            pl.when(place.exists(1))(lambda: whole(ZU, level, tp).start())
        if offset >= 0:
            pl.when(place.exists(-1))(lambda: whole(ZD, level, tp).start())
        whole(X, level, tp).start()
        whole(Y, level, tp).start()
        pair_copy(level, tp, c).start()
        put_out(level, tp, c).start()

    def second(offset):
        level = z + offset
        whole(X, level, place.tx).wait_recv()
        part(DY, level, place.tx).start()
        pair_copy(level, place.tx, c).start()
        put_out(level, place.tx, c).start()
        whole(Y, level, place.ty).wait_recv()
        part(DX, level, place.ty).start()
        pair_copy(level, place.ty, c).start()
        put_out(level, place.ty, c).start()

    def third(offset):
        level = z + offset
        part(DY, level, place.td).wait_recv()
        part(DX, level, place.td).wait_recv()
        pair_copy(level, place.td, c).start()
        put_out(level, place.td, c).start()

    order = place.offsets()
    stages = ((first, 0), (second, 1), (third, 2))
    for step in range(place.levels + 2):
        for stage, lag in stages:
            for offset in order:
                if abs(offset) == step - lag:
                    pl.when(place.exists(offset))(functools.partial(stage, offset))
        if step == 0:
            for hop in range(1, sp_count):
                meta_copy(hop).start()

    pairs = [(level, tile) for level in range(place.levels) for tile in range(tiles)]
    for level, tile in pairs:
        pair_copy(level, tile, 1 - c).wait_recv()
        put_out(level, tile, 1 - c).start()
    for hop in range(1, sp_count):
        meta_copy(hop).wait_send()
        meta_copy(hop).wait_recv()

    def sent(offset):
        level = z + offset
        if offset <= 0:
            pl.when(place.exists(1))(lambda: whole(ZU, level, tp).wait_send())
        if offset >= 0:
            pl.when(place.exists(-1))(lambda: whole(ZD, level, tp).wait_send())
        whole(X, level, tp).wait_send()
        whole(Y, level, tp).wait_send()
        part(DY, level, place.tx).wait_send()
        part(DX, level, place.ty).wait_send()

    for offset in order:
        pl.when(place.exists(offset))(functools.partial(sent, offset))
    for level, tile in pairs:
        pair_copy(level, tile, c).wait_send()
        put_out(level, tile, c).wait()
        put_out(level, tile, 1 - c).wait()


def gather_all(own, meta, sp_count, tp_count):
    rows, cols = own.shape
    levels = sp_count // CORES
    vmem = pl.BlockSpec(memory_space=pltpu.VMEM)
    return pl.pallas_call(
        gather_kernel,
        out_shape=(
            jax.ShapeDtypeStruct((sp_count * rows, tp_count * cols), own.dtype),
            jax.ShapeDtypeStruct((sp_count,) + meta.shape, meta.dtype),
        ),
        in_specs=[vmem, vmem],
        out_specs=(pl.BlockSpec(memory_space=pl.ANY), vmem),
        scratch_shapes=[
            pltpu.VMEM((sp_count * rows, tp_count * cols), own.dtype),
            pltpu.SemaphoreType.DMA((6, levels)),
            pltpu.SemaphoreType.DMA((6, levels)),
            pltpu.SemaphoreType.DMA((levels, tp_count)),
            pltpu.SemaphoreType.DMA((levels, tp_count)),
            pltpu.SemaphoreType.DMA((sp_count,)),
            pltpu.SemaphoreType.DMA((sp_count,)),
            pltpu.SemaphoreType.DMA((2,)),
            pltpu.SemaphoreType.DMA((levels, tp_count, CORES)),
        ],
        compiler_params=pltpu.CompilerParams(collective_id=0, has_side_effects=True),
        name="gather_all",
    )(own, meta)


def combine_kernel(
    part_ref, after_ref, out_ref,
    own_part, r_pair, s_diag, r_ydiag, r_xdiag, s_x, s_y, r_x, r_y, s_z, r_up, r_down,
    send_sem, recv_sem, p_send, p_recv, own_sem,
):
    place = Place(send_sem, recv_sem)
    rows, cols = after_ref.shape
    half = rows // 2
    z, c, tp = place.z, place.c, place.tp
    chunk = 32

    pl.when(z == 0)(lambda: r_up.__setitem__(Ellipsis, jnp.zeros_like(r_up)))
    pl.when(z == place.levels - 1)(lambda: r_down.__setitem__(Ellipsis, jnp.zeros_like(r_down)))
    greet(place, False)

    def pair_copy(level):
        start = pl.multiple_of((level * CORES + (1 - c)) * rows, rows)
        return pltpu.make_async_remote_copy(
            src_ref=part_ref.at[pl.ds(start, rows)],
            dst_ref=r_pair.at[level],
            send_sem=p_send.at[level],
            recv_sem=p_recv.at[level],
            device_id=place.partner,
            device_id_type=MESH,
        )

    def summed(level, tile, row, count=chunk):
        at = pl.ds(pl.multiple_of(row, chunk), count)
        lanes = pl.ds(pl.multiple_of(tile * cols, cols), cols)
        mine = own_part[level, at, lanes].astype(jnp.float32)
        return mine + r_pair[level, at, lanes].astype(jnp.float32)

    def own_copy(level):
        start = pl.multiple_of((level * CORES + c) * rows, rows)
        return pltpu.make_async_copy(
            part_ref.at[pl.ds(start, rows)], own_part.at[level], own_sem.at[level]
        )

    def over(first, last, body):
        def step(index, carry):
            body(pl.multiple_of(first + index * chunk, chunk))
            return carry

        lax.fori_loop(0, (last - first) // chunk, step, 0)

    def diag(kind, level):
        if kind == DY:
            return place.copy(kind, level, s_diag.at[level, pl.ds(0, half)], r_ydiag.at[level])
        return place.copy(kind, level, s_diag.at[level, pl.ds(half, half)], r_xdiag.at[level])

    def side(kind, level):
        if kind == X:
            return place.copy(kind, level, s_x.at[level], r_x.at[level])
        return place.copy(kind, level, s_y.at[level], r_y.at[level])

    def line(kind, level):
        return place.copy(kind, level, s_z.at[level], (r_up if kind == ZU else r_down).at[level])

    def first(offset):
        level = z + offset
        pair_copy(level).wait_recv()
        own_copy(level).wait()

        def body(row):
            s_diag[level, pl.ds(row, chunk)] = summed(level, place.td, row).astype(jnp.bfloat16)

        over(0, half, body)
        diag(DY, level).start()
        over(half, rows, body)
        diag(DX, level).start()

    def second(offset):
        level = z + offset

        def plain(buffer, tile):
            def body(row):
                buffer[level, pl.ds(row, chunk)] = summed(level, tile, row).astype(jnp.bfloat16)

            return body

        def joined(buffer, tile, arrived, base):
            def body(row):
                other = arrived[level, pl.ds(pl.multiple_of(row - base, chunk), chunk)]
                total = summed(level, tile, row) + other.astype(jnp.float32)
                buffer[level, pl.ds(row, chunk)] = total.astype(jnp.bfloat16)

            return body

        over(half, rows, plain(s_x, place.tx))
        over(0, half, plain(s_y, place.ty))
        diag(DY, level).wait_recv()
        over(0, half, joined(s_x, place.tx, r_ydiag, 0))
        side(X, level).start()
        diag(DX, level).wait_recv()
        over(half, rows, joined(s_y, place.ty, r_xdiag, half))
        side(Y, level).start()

    def third(offset):
        level = z + offset
        side(X, level).wait_recv()
        side(Y, level).wait_recv()
        if offset >= 0:
            pl.when(z > 0)(lambda: line(ZU, level).wait_recv())
        if offset <= 0:
            pl.when(z < place.levels - 1)(lambda: line(ZD, level).wait_recv())

        def body(row):
            at = pl.ds(row, chunk)
            total = summed(level, tp, row)
            total = total + r_x[level, at].astype(jnp.float32) + r_y[level, at].astype(jnp.float32)
            if offset >= 0:
                total = total + r_up[level, at].astype(jnp.float32)
            if offset <= 0:
                total = total + r_down[level, at].astype(jnp.float32)
            if offset == 0:
                total = total + after_ref[at].astype(jnp.float32)
                lanes = pl.ds(pl.multiple_of(tp * cols, cols), cols)
                out_ref[at, lanes] = total.astype(jnp.bfloat16)
            else:
                s_z[level, at] = total.astype(jnp.bfloat16)

        over(0, rows, body)
        if offset > 0:
            line(ZU, level).start()
        if offset < 0:
            line(ZD, level).start()

    order = place.offsets()[::-1]
    for offset in order:
        pl.when(place.exists(offset))(lambda offset=offset: pair_copy(z + offset).start())
        pl.when(place.exists(offset))(lambda offset=offset: own_copy(z + offset).start())
    stages = ((first, 0), (second, 1), (third, 4))
    for step in range(len(order) + 4):
        for stage, lag in stages:
            if 0 <= step - lag < len(order):
                offset = order[step - lag]
                pl.when(place.exists(offset))(functools.partial(stage, offset))

    def final(kind, tile):
        start, count = {FX: (0, rows), FY: (0, rows), FDY: (0, half), FDX: (half, half)}[kind]
        ref = out_ref.at[pl.ds(start, count), pl.ds(pl.multiple_of(tile * cols, cols), cols)]
        return place.copy(kind, 0, ref, ref)

    final(FX, tp).start()
    final(FY, tp).start()

    def sent(offset):
        level = z + offset
        pair_copy(level).wait_send()
        for kind in (DX, DY):
            diag(kind, level).wait_send()
        for kind in (X, Y):
            side(kind, level).wait_send()
        if offset > 0:
            line(ZU, level).wait_send()
        if offset < 0:
            line(ZD, level).wait_send()

    final(FX, place.tx).wait_recv()
    final(FDY, place.tx).start()
    final(FY, place.ty).wait_recv()
    final(FDX, place.ty).start()
    for offset in order:
        pl.when(place.exists(offset))(functools.partial(sent, offset))
    final(FDY, place.td).wait_recv()
    final(FDX, place.td).wait_recv()
    final(FX, tp).wait_send()
    final(FY, tp).wait_send()
    final(FDY, place.tx).wait_send()
    final(FDX, place.ty).wait_send()


def combine_all(parts, after, sp_count, tp_count):
    rows, cols = after.shape
    levels = sp_count // CORES
    vmem = pl.BlockSpec(memory_space=pltpu.VMEM)
    whole = pltpu.VMEM((levels, rows, cols), jnp.bfloat16)
    halved = pltpu.VMEM((levels, rows // 2, cols), jnp.bfloat16)
    return pl.pallas_call(
        combine_kernel,
        out_shape=jax.ShapeDtypeStruct((rows, tp_count * cols), after.dtype),
        in_specs=[pl.BlockSpec(memory_space=pl.ANY), vmem],
        out_specs=vmem,
        scratch_shapes=[
            pltpu.VMEM((levels, rows, tp_count * cols), jnp.bfloat16),
            pltpu.VMEM((levels, rows, tp_count * cols), jnp.bfloat16),
            whole, halved, halved, whole, whole, whole, whole, whole, whole, whole,
            pltpu.SemaphoreType.DMA((10, levels)),
            pltpu.SemaphoreType.DMA((10, levels)),
            pltpu.SemaphoreType.DMA((levels,)),
            pltpu.SemaphoreType.DMA((levels,)),
            pltpu.SemaphoreType.DMA((levels,)),
        ],
        compiler_params=pltpu.CompilerParams(collective_id=1, has_side_effects=True),
        name="combine_all",
    )(parts, after)


def shards(
    residual_in,
    mix_gain,
    pool_weight,
    pool_scale,
    ffn_gain,
    route_ids,
    route_weights,
    gate_weight,
    up_weight,
    down_weight,
):
    tp_count = lax.axis_size("tp")
    sp_count = lax.axis_size("sp")
    tp_index = lax.axis_index("tp")
    tok_count, width = residual_in.shape
    group_width = width // GROUPS
    col_count = pool_weight.shape[1]
    block_rows = tok_count // tp_count
    capacity = 2 * TOP_K * block_rows // sp_count
    group_index = tp_index * col_count // group_width
    window = jnp.power(2, group_index + 1)
    stream = residual_in.astype(jnp.float32)
    inverse = lax.rsqrt(jnp.mean(stream * stream, axis=-1, keepdims=True) + EPS)
    stream_group = lax.dynamic_slice_in_dim(residual_in, group_index * group_width, group_width, 1)
    stream_group = stream_group.astype(jnp.float32)
    gain_group = lax.dynamic_slice_in_dim(mix_gain, group_index * group_width, group_width, 0)
    normed_group = (stream_group * inverse * gain_group).astype(jnp.bfloat16)
    rim_rows = from_behind(normed_group[tok_count - SPAN :], "sp", 1)
    extended = jnp.concatenate([rim_rows, normed_group], axis=0).astype(jnp.float32)
    window_sum = jnp.zeros((tok_count, group_width), jnp.float32)
    for offset in range(SPAN):
        window_sum = window_sum + jnp.where(
            offset < window, extended[SPAN - offset : SPAN - offset + tok_count], 0.0
        )
    position = lax.axis_index("sp") * tok_count + jnp.arange(tok_count, dtype=jnp.int32)
    divisor = jnp.minimum(position + 1, window).astype(jnp.float32)
    pooled = (window_sum / divisor[:, None] - extended[SPAN:]).astype(jnp.bfloat16)
    mixed = (jnp.dot(pooled, pool_weight, preferred_element_type=jnp.float32) * pool_scale).astype(
        jnp.bfloat16
    )
    stream_own = lax.dynamic_slice_in_dim(residual_in, tp_index * col_count, col_count, 1)
    after_own = (stream_own.astype(jnp.float32) + mixed.astype(jnp.float32)).astype(jnp.bfloat16)

    meta = jnp.concatenate(
        [
            route_ids.astype(jnp.float32).T,
            route_weights.T,
            jnp.zeros((8 - 2 * TOP_K, tok_count), jnp.float32),
        ],
        axis=0,
    )
    after_all, meta_all = gather_all(after_own, meta, sp_count, tp_count)

    expert = lax.axis_index("sp").astype(jnp.float32)
    named = (meta_all[:, :TOP_K] == expert).astype(jnp.float32)
    match = jnp.sum(named, axis=1)
    weight = jnp.sum(named * meta_all[:, TOP_K : 2 * TOP_K], axis=1)
    at = jnp.arange(tok_count, dtype=jnp.int32)
    earlier = (at[:, None] < at[None, :]) & (at[:, None] // block_rows == at[None, :] // block_rows)
    before = jnp.dot(
        match.astype(jnp.bfloat16),
        earlier.astype(jnp.bfloat16),
        preferred_element_type=jnp.float32,
    )
    slots = capacity * tp_count
    slot_of = before + (at // block_rows * capacity).astype(jnp.float32)[None, :]
    slot_of = jnp.where(match > 0, slot_of, -1.0)
    chosen = slot_of[:, None, :] == jnp.arange(slots, dtype=jnp.float32)[None, :, None]
    table = chosen.astype(jnp.bfloat16)
    slot_weight = jnp.sum(jnp.where(chosen, weight[:, None, :], 0.0), axis=-1).reshape(-1, 1)
    picked = lax.dot_general(
        table,
        after_all.reshape(sp_count, tok_count, width),
        (((2,), (1,)), ((0,), (0,))),
        preferred_element_type=jnp.float32,
    ).reshape(-1, width)
    flat_rows = rms_scale(picked, ffn_gain).astype(jnp.bfloat16)
    gate_part = jnp.dot(flat_rows, gate_weight[0], preferred_element_type=jnp.float32)
    up_part = jnp.dot(flat_rows, up_weight[0], preferred_element_type=jnp.float32)
    hidden = (jax.nn.silu(gate_part) * up_part).astype(jnp.bfloat16)
    term = jnp.dot(hidden, down_weight[0], preferred_element_type=jnp.float32)
    term = (term * slot_weight).astype(jnp.bfloat16)
    parts = lax.dot_general(
        table,
        term.reshape(sp_count, slots, width),
        (((1,), (1,)), ((0,), (0,))),
        preferred_element_type=jnp.float32,
    ).astype(jnp.bfloat16)
    return combine_all(parts.reshape(-1, width), after_own, sp_count, tp_count)


def solution(mesh):
    placed = (
        P("sp", None),
        P(),
        P(None, "tp"),
        P("tp"),
        P(),
        P("sp", None),
        P("sp", None),
        P("sp", None, "tp"),
        P("sp", None, "tp"),
        P("sp", "tp", None),
    )
    square = mesh.shape["tp"] == SIDE * SIDE and mesh.shape["sp"] % CORES == 0
    return jax.shard_map(
        shards if square else shards_any,
        mesh=mesh,
        in_specs=placed,
        out_specs=P("sp", None),
        check_vma=False,
    )
```

profile of v0, /device:TPU:0, one launch (start us, length us, event | category | flops | bytes accessed | tf_op | source)
XLA Modules:
  0.0 148.0 jit_solution(1338274280427192576)
XLA Ops:
  0.0 0.0 copy-start
  0.0 1.6 %multiply_reduce_fusion.1 = f32[256]{0:T(256)S(1)} fusion(bf16[256,2048]{1,0:T(8,128)(2,1)} %param.10), kind=kLoop, calls=%fused_computation.10 | loop fusion | flops 1572608 | bytes 1049600 | tf_op jit(solution)/shard_map/reduce_sum | solution.py:569
  1.6 0.8 dynamic_slice.11
  2.4 1.1 multiply_convert_fusion.3
  3.4 2.4 %collective-permute-start = (bf16[16,512]{1,0:T(8,128)(2,1)S(1)}, bf16[16,512]{1,0:T(8,128)(2,1)S(1)}, u32[]{:S(2)}, u32[]{:S(2)}) collective-permute-start(bf16[16,512]{1,0:T(8,128)(2,1)S(1)} %slice.77), channel_id=1, source_target_pairs={{0,4},{4,8},{8,12},{12,16},{16,20},{20,24},{24,28},{1,5},{5,9},{9,... | collective-permute-start | bytes 49160 | tf_op jit(solution)/shard_map/ppermute | solution.py:22
  5.9 0.7 convert_bitcast_fusion
  6.6 0.1 pad.2.clone
  6.7 1.3 maximum_maximum_fusion.meta_ref
  8.0 0.0 collective-permute-done
  8.0 0.1 maximum_convert_fusion
  8.1 0.0 copy-done
  8.1 3.0 %fusion.10.own_ref.after_ref = bf16[256,512]{1,0:T(8,128)(2,1)} fusion(bf16[512,512]{1,0:T(8,128)(2,1)S(1)} %copy-done, f32[512]{0:T(512)} %param.13, bf16[256,2048]{1,0:T(8,128)(2,1)} %param.10, s32[]{:T(128)S(6)} %select_n.166, f32[272,512]{1,0:T(8,128)S(1)} %maximum_convert_fusion, f32[256]{0:T(256)S(1)} %minimum_convert_fusion, pred[]{:T(512)S(6)} %gt.69, ...), kind=kOutput, calls=%fused_computation.15 | convolution fusion | flops 139460608 | bytes 9440276 | tf_op jit(solution)/shard_map/dot_general | solution.py:584
  11.1 48.1 %gather_all.1 = (bf16[2048,2048]{1,0:T(8,128)(2,1)}, f32[8,8,256]{2,1,0:T(8,128)}) custom-call(bf16[256,512]{1,0:T(8,128)(2,1)} %fusion.10.own_ref.after_ref, f32[8,256]{1,0:T(8,128)} %maximum_maximum_fusion.meta_ref), custom_call_target="tpu_custom_call" | custom-call | tf_op jit(solution)/shard_map/gather_all/pallas_call | solution.py:324
  59.1 1.0 select_reduce_fusion.1
  60.1 0.2 fusion.11
  60.3 0.6 select_reduce_fusion
  61.0 0.0 copy-start.1
  61.0 4.6 %multiply_reduce_fusion = (f32[8,128]{1,0:T(8,128)S(1)}, f32[8,128,2048]{2,1,0:T(8,128)S(1)}) fusion(bf16[8,256,2048]{2,1,0:T(8,128)(2,1)} %bitcast.26, f32[8,256]{1,0:T(8,128)S(1)} %fusion.11), kind=kOutput, calls=%fused_computation.2 | convolution fusion | flops 1078197248 | bytes 16789504 | tf_op jit(solution)/shard_map/dot_general | solution.py:617
  65.6 0.0 copy-done.1
  65.6 0.0 copy-start.2
  65.7 0.8 multiply_convert_fusion.1
  66.4 1.2 copy-done.2
  67.7 0.0 copy-start.3
  67.7 4.5 %fusion.1 = f32[1024,896]{1,0:T(8,128)S(1)} fusion(bf16[1024,2048]{1,0:T(8,128)(2,1)S(1)} %bitcast.28, bf16[1,2048,896]{2,1,0:T(8,128)(2,1)S(1)} %copy-done.2), kind=kOutput, calls=%fused_computation.5 | convolution fusion | flops 3758096384 | bytes 11534336 | tf_op jit(solution)/shard_map/dot_general | solution.py:625
  72.2 0.0 copy-done.3
  72.2 0.0 copy-start.4
  72.2 4.8 %multiply_convert_fusion.2 = bf16[1024,896]{1,0:T(8,128)(2,1)S(1)} fusion(f32[1024,896]{1,0:T(8,128)S(1)} %fusion.1, bf16[1024,2048]{1,0:T(8,128)(2,1)S(1)} %bitcast.29, bf16[1,2048,896]{2,1,0:T(8,128)(2,1)S(1)} %copy-done.3), kind=kOutput, calls=%fused_computation.9 | convolution fusion | flops 3763601408 | bytes 13369344 | tf_op jit(solution)/shard_map/dot_general | solution.py:624
  77.0 0.0 copy-done.4
  77.0 4.7 %multiply_convert_fusion = bf16[1024,2048]{1,0:T(8,128)(2,1)S(1)} fusion(bf16[1024,896]{1,0:T(8,128)(2,1)S(1)} %multiply_convert_fusion.2, f32[1024]{0:T(1024)S(1)} %bitcast.30, bf16[1,896,2048]{2,1,0:T(8,128)(2,1)S(1)} %copy-done.4), kind=kOutput, calls=%fused_computation | convolution fusion | flops 3762290688 | bytes 9703424 | tf_op jit(solution)/shard_map/dot_general | solution.py:627
  81.7 5.6 %convolution_convert_fusion = bf16[8,256,2048]{2,1,0:T(8,128)(2,1)} fusion(bf16[8,128,2048]{2,1,0:T(8,128)(2,1)S(1)} %bitcast.27, f32[8,256]{1,0:T(8,128)S(1)} %fusion.11), kind=kOutput, calls=%fused_computation.3 | convolution fusion | flops 1078198272 | bytes 12591104 | tf_op jit(solution)/shard_map/dot_general | solution.py:629
  87.3 58.4 %combine_all.1 = bf16[256,2048]{1,0:T(8,128)(2,1)} custom-call(bf16[2048,2048]{1,0:T(8,128)(2,1)} %bitcast.25, bf16[256,512]{1,0:T(8,128)(2,1)} %fusion.10.own_ref.after_ref), custom_call_target="tpu_custom_call" | custom-call | tf_op jit(solution)/shard_map/combine_all/pallas_call | solution.py:526
  145.7 2.3 %copy.14 = bf16[256,2048]{1,0:T(8,128)(2,1)} copy(bf16[256,2048]{1,0:T(8,128)(2,1)} %combine_all.1) | data formatting | bytes 2097152
  (6 shorter events, 0.0 us)
Async XLA Ops:
  0.0 8.1 %copy-start = (bf16[512,512]{1,0:T(8,128)(2,1)S(1)}, bf16[512,512]{1,0:T(8,128)(2,1)}, u32[]{:S(2)}) copy-start(bf16[512,512]{1,0:T(8,128)(2,1)} %param.12) | copy-start | bytes 1572868
  3.4 4.6 %collective-permute-start = (bf16[16,512]{1,0:T(8,128)(2,1)S(1)}, bf16[16,512]{1,0:T(8,128)(2,1)S(1)}, u32[]{:S(2)}, u32[]{:S(2)}) collective-permute-start(bf16[16,512]{1,0:T(8,128)(2,1)S(1)} %slice.77), channel_id=1, source_target_pairs={{0,4},{4,8},{8,12},{12,16},{16,20},{20,24},{24,28},{1,5},{5,9},{9,... | collective-permute-start | bytes 49160 | tf_op jit(solution)/shard_map/ppermute | solution.py:22
  61.0 4.7 %copy-start.1 = (f32[2048]{0:T(1024)S(1)}, f32[2048]{0:T(1024)}, u32[]{:S(2)}) copy-start(f32[2048]{0:T(1024)} %param.14) | copy-start | bytes 24580
  65.6 2.0 %copy-start.2 = (bf16[1,2048,896]{2,1,0:T(8,128)(2,1)S(1)}, bf16[1,2048,896]{2,1,0:T(8,128)(2,1)}, u32[]{:S(2)}) copy-start(bf16[1,2048,896]{2,1,0:T(8,128)(2,1)} %param.18) | copy-start | bytes 11010052
  67.7 4.5 %copy-start.3 = (bf16[1,2048,896]{2,1,0:T(8,128)(2,1)S(1)}, bf16[1,2048,896]{2,1,0:T(8,128)(2,1)}, u32[]{:S(2)}) copy-start(bf16[1,2048,896]{2,1,0:T(8,128)(2,1)} %param.17) | copy-start | bytes 11010052
  72.2 4.8 %copy-start.4 = (bf16[1,896,2048]{2,1,0:T(8,128)(2,1)S(1)}, bf16[1,896,2048]{2,1,0:T(8,128)(2,1)}, u32[]{:S(2)}) copy-start(bf16[1,896,2048]{2,1,0:T(8,128)(2,1)} %param.19) | copy-start | bytes 11010052
where the time goes:
time: 148 us
  Pallas kernels  106 us (72%)
  matrix products  27.4 us (19%)
  other arithmetic  7.13 us (5%)
  local copies, waits for them, and re-layouts  4.42 us (3%)
  starting transfers between devices  2.4 us (2%)
    pallas_call x1, Pallas kernels, combine_all(): pl.pallas_call(combine_kernel, out_shape=jax.ShapeDtypeStruct((rows, tp_c...  58.4 us
    pallas_call x1, Pallas kernels, gather_all(): pl.pallas_call(gather_kernel, out_shape=(jax.ShapeDtypeStruct((sp_count *...  48.1 us
    dot_general x1, matrix products, shards(): lax.dot_general(table, term.reshape(sp_count, slots, width), (((1,), (1,)...  5.59 us
    dot_general x1, matrix products, shards(): jnp.dot(flat_rows, gate_weight[0], preferred_element_type=jnp.float32)  4.77 us
    dot_general x1, matrix products, shards(): term = jnp.dot(hidden, down_weight[0], preferred_element_type=jnp.float32)  4.71 us
    dot_general x1, matrix products, shards(): lax.dot_general(table, after_all.reshape(sp_count, tok_count, width), (((...  4.64 us
    dot_general x1, matrix products, shards(): jnp.dot(flat_rows, up_weight[0], preferred_element_type=jnp.float32)  4.49 us
    unnamed x11, local copies, waits for them, and re-layouts  3.57 us
  transfers between devices with their start and end apart: 1, of which 0 were waited for; matrix products, arithmetic and copies ran while one was open for 1% of the time, Pallas kernels for 0%

commit v1 on v0

--- a/solution.py
+++ b/solution.py
@@ -12,6 +12,7 @@
 TOP_K = 2
 CORES = 2
 SIDE = 2
+LANES = 128
 EPS = 1e-06
 MESH = pl.DeviceIdType.MESH
 ZU, ZD, X, Y, DX, DY, FX, FY, FDX, FDY = range(10)
@@ -178,10 +179,9 @@
         pl.semaphore_wait(barrier, count + 1)
     else:
         hello(place.partner)
-        up, down = place.exists(1), place.exists(-1)
-        pl.when(up)(lambda: hello(place.to[ZU]))
-        pl.when(down)(lambda: hello(place.to[ZD]))
-        pl.semaphore_wait(barrier, 3 + up.astype(jnp.int32) + down.astype(jnp.int32))
+        for step in range(1, place.levels):
+            hello((lax.rem(place.z + step, place.levels) * CORES + place.c, place.tp))
+        pl.semaphore_wait(barrier, place.levels + 2)
 
 
 def gather_kernel(
@@ -345,25 +345,65 @@
     )(own, meta)
 
 
-def combine_kernel(
-    part_ref, after_ref, out_ref,
-    own_part, r_pair, s_diag, r_ydiag, r_xdiag, s_x, s_y, r_x, r_y, s_z, r_up, r_down,
-    send_sem, recv_sem, p_send, p_recv, own_sem,
+def level_order(place):
+    everywhere = range(place.levels)
+    orders = []
+    for z in everywhere:
+        offsets = [offset for offset in place.offsets()[::-1] if 0 <= z + offset < place.levels]
+        orders.append([z + offset for offset in offsets])
+    steps = []
+    for index in everywhere:
+        level = jnp.int32(orders[0][index])
+        for z in everywhere[1:]:
+            level = jnp.where(place.z == z, orders[z][index], level)
+        steps.append(level)
+    return steps
+
+
+def experts_kernel(
+    rows_ref, slot_ref, weight_ref, gain_ref, gate_ref, up_ref, down_ref, after_ref, out_ref,
+    held, gu, dn, picked, hid, spread, scale, parts,
+    r_pair, s_diag, r_ydiag, r_xdiag, s_x, s_y, r_x, r_y, s_z, r_z,
+    send_sem, recv_sem, p_send, p_recv, z_send, z_recv, h_sem, w_sem,
 ):
     place = Place(send_sem, recv_sem)
     rows, cols = after_ref.shape
+    width = rows_ref.shape[1]
+    slots = spread.shape[2]
     half = rows // 2
     z, c, tp = place.z, place.c, place.tp
     chunk = 32
-
-    pl.when(z == 0)(lambda: r_up.__setitem__(Ellipsis, jnp.zeros_like(r_up)))
-    pl.when(z == place.levels - 1)(lambda: r_down.__setitem__(Ellipsis, jnp.zeros_like(r_down)))
+    pieces, _, pair_lanes = gu.shape
+    lanes_each = pair_lanes // 2
+    order = level_order(place)
+    wide = 256
+
+    def held_copy(level):
+        at = pl.ds(pl.multiple_of(level * CORES * rows, CORES * rows), CORES * rows)
+        return pltpu.make_async_copy(rows_ref.at[at], held.at[level], h_sem.at[level])
+
+    def gate_copy(piece, side):
+        source = (gate_ref, up_ref)[side]
+        return pltpu.make_async_copy(
+            source.at[0, :, pl.ds(piece * lanes_each, lanes_each)],
+            gu.at[piece, :, pl.ds(side * lanes_each, lanes_each)],
+            w_sem.at[piece, side],
+        )
+
+    down_copy = pltpu.make_async_copy(down_ref.at[0], dn, w_sem.at[pieces, 0])
+
+    held_copy(order[0]).start()
+    for piece in range(pieces):
+        gate_copy(piece, 0).start()
+        gate_copy(piece, 1).start()
+    down_copy.start()
+    for level in order[1:]:
+        held_copy(level).start()
     greet(place, False)
 
     def pair_copy(level):
-        start = pl.multiple_of((level * CORES + (1 - c)) * rows, rows)
         return pltpu.make_async_remote_copy(
-            src_ref=part_ref.at[pl.ds(start, rows)],
+            src_ref=parts.at[level, 1 - c],
             dst_ref=r_pair.at[level],
             send_sem=p_send.at[level],
             recv_sem=p_recv.at[level],
@@ -371,17 +411,61 @@
             device_id_type=MESH,
         )
 
+    def pick(level):
+        held_copy(level).wait()
+        for b in range(CORES):
+            slot = slot_ref[level * CORES + b]
+            weight = weight_ref[level * CORES + b]
+            at = lax.broadcasted_iota(jnp.int32, (slots, rows), 0).astype(jnp.float32)
+            chosen = at == slot
+            table = jnp.where(chosen, 1.0, 0.0)
+            scale[b] = jnp.sum(jnp.where(chosen, weight, 0.0), axis=1, keepdims=True)
+            spread[b] = table.T.astype(jnp.bfloat16)
+            table = table.astype(jnp.bfloat16)
+            squares = jnp.zeros((slots, 1), jnp.float32)
+            into = slice(b * slots, (b + 1) * slots)
+            for start in range(0, width, wide):
+                lanes = slice(start, start + wide)
+                value = jnp.dot(
+                    table,
+                    held[level, b * rows : (b + 1) * rows, lanes],
+                    preferred_element_type=jnp.float32,
+                )
+                squares = squares + jnp.sum(value * value, axis=1, keepdims=True)
+                picked[into, lanes] = value.astype(jnp.bfloat16)
+            inverse = lax.rsqrt(squares / width + EPS)
+            for start in range(0, width, wide):
+                lanes = slice(start, start + wide)
+                value = picked[into, lanes].astype(jnp.float32) * inverse * gain_ref[:, lanes]
+                picked[into, lanes] = value.astype(jnp.bfloat16)
+
+    def grow(first_time):
+        for piece in range(pieces):
+            if first_time:
+                gate_copy(piece, 0).wait()
+                gate_copy(piece, 1).wait()
+            both = jnp.dot(picked[...], gu[piece], preferred_element_type=jnp.float32)
+            gate, up = both[:, :lanes_each], both[:, lanes_each:]
+            lanes = slice(piece * lanes_each, (piece + 1) * lanes_each)
+            hid[:, lanes] = (jax.nn.silu(gate) * up).astype(jnp.bfloat16)
+
+    def shrink(level, first_time):
+        if first_time:
+            down_copy.wait()
+        for start in range(0, width, 2 * wide):
+            lanes = slice(start, start + 2 * wide)
+            term = jnp.dot(hid[...], dn[:, lanes], preferred_element_type=jnp.float32)
+            for b in range(CORES):
+                scaled = (term[b * slots : (b + 1) * slots] * scale[b]).astype(jnp.bfloat16)
+                value = jnp.dot(spread[b], scaled, preferred_element_type=jnp.float32)
+                parts[level, b, :, lanes] = value.astype(jnp.bfloat16)
+        pair_copy(level).start()
+
     def summed(level, tile, row, count=chunk):
         at = pl.ds(pl.multiple_of(row, chunk), count)
         lanes = pl.ds(pl.multiple_of(tile * cols, cols), cols)
-        mine = own_part[level, at, lanes].astype(jnp.float32)
+        mine = parts[level, c, at, lanes].astype(jnp.float32)
         return mine + r_pair[level, at, lanes].astype(jnp.float32)
-
-    def own_copy(level):
-        start = pl.multiple_of((level * CORES + c) * rows, rows)
-        return pltpu.make_async_copy(
-            part_ref.at[pl.ds(start, rows)], own_part.at[level], own_sem.at[level]
-        )
 
     def over(first, last, body):
         def step(index, carry):
@@ -400,13 +484,28 @@
             return place.copy(kind, level, s_x.at[level], r_x.at[level])
         return place.copy(kind, level, s_y.at[level], r_y.at[level])
 
-    def line(kind, level):
-        return place.copy(kind, level, s_z.at[level], (r_up if kind == ZU else r_down).at[level])
-
-    def first(offset):
-        level = z + offset
+    def line(level):
+        return pltpu.make_async_remote_copy(
+            src_ref=s_z.at[level],
+            dst_ref=r_z.at[z],
+            send_sem=z_send.at[level],
+            recv_sem=z_recv.at[z],
+            device_id=(level * CORES + c, tp),
+            device_id_type=MESH,
+        )
+
+    def line_arrival(level):
+        return pltpu.make_async_remote_copy(
+            src_ref=s_z.at[level],
+            dst_ref=r_z.at[level],
+            send_sem=z_send.at[level],
+            recv_sem=z_recv.at[level],
+            device_id=(level * CORES + c, tp),
+            device_id_type=MESH,
+        )
+
+    def first(level):
         pair_copy(level).wait_recv()
-        own_copy(level).wait()
 
         def body(row):
             s_diag[level, pl.ds(row, chunk)] = summed(level, place.td, row).astype(jnp.bfloat16)
@@ -416,9 +515,7 @@
         over(half, rows, body)
         diag(DX, level).start()
 
-    def second(offset):
-        level = z + offset
-
+    def second(level):
         def plain(buffer, tile):
             def body(row):
                 buffer[level, pl.ds(row, chunk)] = summed(level, tile, row).astype(jnp.bfloat16)
@@ -442,46 +539,54 @@
         over(half, rows, joined(s_y, place.ty, r_xdiag, half))
         side(Y, level).start()
 
-    def third(offset):
-        level = z + offset
+    def third(level):
         side(X, level).wait_recv()
         side(Y, level).wait_recv()
-        if offset >= 0:
-            pl.when(z > 0)(lambda: line(ZU, level).wait_recv())
-        if offset <= 0:
-            pl.when(z < place.levels - 1)(lambda: line(ZD, level).wait_recv())
 
         def body(row):
             at = pl.ds(row, chunk)
             total = summed(level, tp, row)
             total = total + r_x[level, at].astype(jnp.float32) + r_y[level, at].astype(jnp.float32)
-            if offset >= 0:
-                total = total + r_up[level, at].astype(jnp.float32)
-            if offset <= 0:
-                total = total + r_down[level, at].astype(jnp.float32)
-            if offset == 0:
-                total = total + after_ref[at].astype(jnp.float32)
-                lanes = pl.ds(pl.multiple_of(tp * cols, cols), cols)
-                out_ref[at, lanes] = total.astype(jnp.bfloat16)
-            else:
-                s_z[level, at] = total.astype(jnp.bfloat16)
+            s_z[level, at] = total.astype(jnp.bfloat16)
 
         over(0, rows, body)
-        if offset > 0:
-            line(ZU, level).start()
-        if offset < 0:
-            line(ZD, level).start()
-
-    order = place.offsets()[::-1]
-    for offset in order:
-        pl.when(place.exists(offset))(lambda offset=offset: pair_copy(z + offset).start())
-        pl.when(place.exists(offset))(lambda offset=offset: own_copy(z + offset).start())
-    stages = ((first, 0), (second, 1), (third, 4))
-    for step in range(len(order) + 4):
-        for stage, lag in stages:
-            if 0 <= step - lag < len(order):
-                offset = order[step - lag]
-                pl.when(place.exists(offset))(functools.partial(stage, offset))
+        line(level).start()
+
+    def finish(level):
+        side(X, level).wait_recv()
+        side(Y, level).wait_recv()
+        for other in order[:-1]:
+            line_arrival(other).wait_recv()
+
+        def body(row):
+            at = pl.ds(row, chunk)
+            total = summed(level, tp, row)
+            total = total + r_x[level, at].astype(jnp.float32) + r_y[level, at].astype(jnp.float32)
+            for other in order[:-1]:
+                total = total + r_z[other, at].astype(jnp.float32)
+            total = total + after_ref[at].astype(jnp.float32)
+            lanes = pl.ds(pl.multiple_of(tp * cols, cols), cols)
+            out_ref[at, lanes] = total.astype(jnp.bfloat16)
+
+        over(0, rows, body)
+
+    last = place.levels - 1
+    for step in range(place.levels + 1):
+        if step <= last:
+            pick(order[step])
+        if step >= 1:
+            first(order[step - 1])
+        if 3 <= step <= last:
+            third(order[step - 3])
+        if step <= last:
+            grow(step == 0)
+        if step >= 1:
+            second(order[step - 1])
+        if step <= last:
+            shrink(order[step], step == 0)
+    for step in range(max(0, last - 2), last):
+        third(order[step])
+    finish(order[last])
 
     def final(kind, tile):
         start, count = {FX: (0, rows), FY: (0, rows), FDY: (0, half), FDX: (half, half)}[kind]
@@ -491,24 +596,21 @@
     final(FX, tp).start()
     final(FY, tp).start()
 
-    def sent(offset):
-        level = z + offset
+    def sent(level, own):
         pair_copy(level).wait_send()
         for kind in (DX, DY):
             diag(kind, level).wait_send()
         for kind in (X, Y):
             side(kind, level).wait_send()
-        if offset > 0:
-            line(ZU, level).wait_send()
-        if offset < 0:
-            line(ZD, level).wait_send()
+        if not own:
+            line(level).wait_send()
 
     final(FX, place.tx).wait_recv()
     final(FDY, place.tx).start()
     final(FY, place.ty).wait_recv()
     final(FDX, place.ty).start()
-    for offset in order:
-        pl.when(place.exists(offset))(functools.partial(sent, offset))
+    for step, level in enumerate(order):
+        sent(level, step == last)
     final(FDY, place.td).wait_recv()
     final(FDX, place.td).wait_recv()
     final(FX, tp).wait_send()
@@ -517,30 +619,47 @@
     final(FDX, place.ty).wait_send()
 
 
-def combine_all(parts, after, sp_count, tp_count):
+def experts_all(after_all, slot_of, weight, gain, gate, up, down, after, capacity, sp_count, tp_count):
     rows, cols = after.shape
+    width = tp_count * cols
+    hidden = gate.shape[2]
     levels = sp_count // CORES
+    slots = capacity * tp_count
     vmem = pl.BlockSpec(memory_space=pltpu.VMEM)
+    hbm = pl.BlockSpec(memory_space=pl.ANY)
     whole = pltpu.VMEM((levels, rows, cols), jnp.bfloat16)
     halved = pltpu.VMEM((levels, rows // 2, cols), jnp.bfloat16)
+    pieces = hidden // LANES
     return pl.pallas_call(
-        combine_kernel,
-        out_shape=jax.ShapeDtypeStruct((rows, tp_count * cols), after.dtype),
-        in_specs=[pl.BlockSpec(memory_space=pl.ANY), vmem],
+        experts_kernel,
+        out_shape=jax.ShapeDtypeStruct((rows, width), after.dtype),
+        in_specs=[hbm, vmem, vmem, vmem, hbm, hbm, hbm, vmem],
         out_specs=vmem,
         scratch_shapes=[
-            pltpu.VMEM((levels, rows, tp_count * cols), jnp.bfloat16),
-            pltpu.VMEM((levels, rows, tp_count * cols), jnp.bfloat16),
-            whole, halved, halved, whole, whole, whole, whole, whole, whole, whole,
+            pltpu.VMEM((levels, CORES * rows, width), jnp.bfloat16),
+            pltpu.VMEM((pieces, width, 2 * LANES), jnp.bfloat16),
+            pltpu.VMEM((hidden, width), jnp.bfloat16),
+            pltpu.VMEM((CORES * slots, width), jnp.bfloat16),
+            pltpu.VMEM((CORES * slots, hidden), jnp.bfloat16),
+            pltpu.VMEM((CORES, rows, slots), jnp.bfloat16),
+            pltpu.VMEM((CORES, slots, 1), jnp.float32),
+            pltpu.VMEM((levels, CORES, rows, width), jnp.bfloat16),
+            pltpu.VMEM((levels, rows, width), jnp.bfloat16),
+            whole, halved, halved, whole, whole, whole, whole, whole, whole,
             pltpu.SemaphoreType.DMA((10, levels)),
             pltpu.SemaphoreType.DMA((10, levels)),
             pltpu.SemaphoreType.DMA((levels,)),
             pltpu.SemaphoreType.DMA((levels,)),
             pltpu.SemaphoreType.DMA((levels,)),
+            pltpu.SemaphoreType.DMA((levels,)),
+            pltpu.SemaphoreType.DMA((levels,)),
+            pltpu.SemaphoreType.DMA((pieces + 1, 2)),
         ],
-        compiler_params=pltpu.CompilerParams(collective_id=1, has_side_effects=True),
-        name="combine_all",
-    )(parts, after)
+        compiler_params=pltpu.CompilerParams(
+            collective_id=1, has_side_effects=True, vmem_limit_bytes=62 * 1024 * 1024
+        ),
+        name="experts_all",
+    )(after_all, slot_of, weight, gain, gate, up, down, after)
 
 
 def shards(
@@ -608,31 +727,21 @@
         earlier.astype(jnp.bfloat16),
         preferred_element_type=jnp.float32,
     )
-    slots = capacity * tp_count
     slot_of = before + (at // block_rows * capacity).astype(jnp.float32)[None, :]
     slot_of = jnp.where(match > 0, slot_of, -1.0)
-    chosen = slot_of[:, None, :] == jnp.arange(slots, dtype=jnp.float32)[None, :, None]
-    table = chosen.astype(jnp.bfloat16)
-    slot_weight = jnp.sum(jnp.where(chosen, weight[:, None, :], 0.0), axis=-1).reshape(-1, 1)
-    picked = lax.dot_general(
-        table,
-        after_all.reshape(sp_count, tok_count, width),
-        (((2,), (1,)), ((0,), (0,))),
-        preferred_element_type=jnp.float32,
-    ).reshape(-1, width)
-    flat_rows = rms_scale(picked, ffn_gain).astype(jnp.bfloat16)
-    gate_part = jnp.dot(flat_rows, gate_weight[0], preferred_element_type=jnp.float32)
-    up_part = jnp.dot(flat_rows, up_weight[0], preferred_element_type=jnp.float32)
-    hidden = (jax.nn.silu(gate_part) * up_part).astype(jnp.bfloat16)
-    term = jnp.dot(hidden, down_weight[0], preferred_element_type=jnp.float32)
-    term = (term * slot_weight).astype(jnp.bfloat16)
-    parts = lax.dot_general(
-        table,
-        term.reshape(sp_count, slots, width),
-        (((1,), (1,)), ((0,), (0,))),
-        preferred_element_type=jnp.float32,
-    ).astype(jnp.bfloat16)
-    return combine_all(parts.reshape(-1, width), after_own, sp_count, tp_count)
+    return experts_all(
+        after_all,
+        slot_of[:, None],
+        weight[:, None],
+        ffn_gain[None],
+        gate_weight,
+        up_weight,
+        down_weight,
+        after_own,
+        capacity,
+        sp_count,
+        tp_count,
+    )
 
 
 def solution(mesh):

time: 148 us -> 140 us (0.946)
  the two profiles are of different devices: /device:TPU:0 before, /device:TPU:18 now
where the time goes in v1:
time: 140 us
  Pallas kernels  123 us (88%)
  other arithmetic  5.71 us (4%)
  local copies, waits for them, and re-layouts  4.36 us (3%)
  matrix products  3.19 us (2%)
  starting transfers between devices  1.92 us (1%)
    pallas_call x1, Pallas kernels, experts_all(): pl.pallas_call(experts_kernel, out_shape=jax.ShapeDtypeStruct((rows, widt...  78.8 us
    pallas_call x1, Pallas kernels, gather_all(): pl.pallas_call(gather_kernel, out_shape=(jax.ShapeDtypeStruct((sp_count *...  44.5 us
    dot_general x1, matrix products, shards(): jnp.dot(pooled, pool_weight, preferred_element_type=jnp.float32)  2.97 us
  transfers between devices with their start and end apart: 1, of which 1 were waited for; matrix products, arithmetic and copies ran while one was open for 2% of the time, Pallas kernels for 0%

profile of v1, /device:TPU:18, one launch (start us, length us, event | category | flops | bytes accessed | tf_op | source)
XLA Modules:
  0.0 139.6 jit_solution(12401908211869215556)
XLA Ops:
  0.0 0.0 copy-start
  0.0 1.6 %multiply_reduce_fusion = f32[256]{0:T(256)S(1)} fusion(bf16[256,2048]{1,0:T(8,128)(2,1)} %param.10), kind=kLoop, calls=%fused_computation | loop fusion | flops 1572608 | bytes 1049600 | tf_op jit(solution)/shard_map/reduce_sum | solution.py:688
  1.6 0.8 dynamic_slice.11
  2.4 1.1 multiply_convert_fusion
  3.4 1.9 %collective-permute-start = (bf16[16,512]{1,0:T(8,128)(2,1)S(1)}, bf16[16,512]{1,0:T(8,128)(2,1)S(1)}, u32[]{:S(2)}, u32[]{:S(2)}) collective-permute-start(bf16[16,512]{1,0:T(8,128)(2,1)S(1)} %slice.77), channel_id=1, source_target_pairs={{0,4},{4,8},{8,12},{12,16},{16,20},{20,24},{24,28},{1,5},{5,9},{9,... | collective-permute-start | bytes 49160 | tf_op jit(solution)/shard_map/ppermute | solution.py:23
  5.4 0.7 convert_bitcast_fusion
  6.1 0.1 pad.2.clone
  6.2 1.3 maximum_maximum_fusion.meta_ref
  7.5 1.0 collective-permute-done
  8.5 0.1 maximum_convert_fusion
  8.6 0.0 copy-done
  8.6 3.0 %fusion.3.own_ref.after_ref = bf16[256,512]{1,0:T(8,128)(2,1)} fusion(bf16[512,512]{1,0:T(8,128)(2,1)S(1)} %copy-done, f32[512]{0:T(512)} %param.13, bf16[256,2048]{1,0:T(8,128)(2,1)} %param.10, s32[]{:T(128)S(6)} %select_n.162, f32[272,512]{1,0:T(8,128)S(1)} %maximum_convert_fusion, f32[256]{0:T(256)S(1)} %minimum_convert_fusion, pred[]{:T(512)S(6)} %gt.69, ...), kind=kOutput, calls=%fused_computation.5 | convolution fusion | flops 139460608 | bytes 9440276 | tf_op jit(solution)/shard_map/dot_general | solution.py:703
  11.5 44.5 %gather_all.1 = (bf16[2048,2048]{1,0:T(8,128)(2,1)}, f32[8,8,256]{2,1,0:T(8,128)}) custom-call(bf16[256,512]{1,0:T(8,128)(2,1)} %fusion.3.own_ref.after_ref, f32[8,256]{1,0:T(8,128)} %maximum_maximum_fusion.meta_ref), custom_call_target="tpu_custom_call" | custom-call | tf_op jit(solution)/shard_map/gather_all/pallas_call | solution.py:324
  56.1 1.0 select_reduce_fusion
  57.0 0.6 broadcast_in_dim.48.weight_ref
  57.6 0.2 fusion.4
  57.8 0.6 broadcast_in_dim.47.slot_ref
  58.5 78.8 %experts_all.1 = bf16[256,2048]{1,0:T(8,128)(2,1)} custom-call(bf16[2048,2048]{1,0:T(8,128)(2,1)} %get-tuple-element.7.rows_ref, f32[8,1,256]{2,1,0:T(1,128)} %broadcast_in_dim.47.slot_ref, f32[8,1,256]{2,1,0:T(1,128)} %broadcast_in_dim.48.weight_ref, f32[1,2048]{1,0:T(1,128)} %bitcast.5, bf16[1,2048,896]{2,1,0:T(8,128)(2,1)} %gate_ref.1, ...), custom_call_target="tpu_custom_call" | custom-call | tf_op jit(solution)/shard_map/experts_all/pallas_call | solution.py:633
  137.3 2.3 %copy.12 = bf16[256,2048]{1,0:T(8,128)(2,1)} copy(bf16[256,2048]{1,0:T(8,128)(2,1)} %experts_all.1) | data formatting | bytes 2097152
  (5 shorter events, 0.0 us)
Async XLA Ops:
  0.0 8.6 %copy-start = (bf16[512,512]{1,0:T(8,128)(2,1)S(1)}, bf16[512,512]{1,0:T(8,128)(2,1)}, u32[]{:S(2)}) copy-start(bf16[512,512]{1,0:T(8,128)(2,1)} %param.12) | copy-start | bytes 1572868
  3.4 5.1 %collective-permute-start = (bf16[16,512]{1,0:T(8,128)(2,1)S(1)}, bf16[16,512]{1,0:T(8,128)(2,1)S(1)}, u32[]{:S(2)}, u32[]{:S(2)}) collective-permute-start(bf16[16,512]{1,0:T(8,128)(2,1)S(1)} %slice.77), channel_id=1, source_target_pairs={{0,4},{4,8},{8,12},{12,16},{16,20},{20,24},{24,28},{1,5},{5,9},{9,... | collective-permute-start | bytes 49160 | tf_op jit(solution)/shard_map/ppermute | solution.py:23

commit v2 on v1

v2 whole, which is shorter than its diff:
```python
import jax
import jax.numpy as jnp
from jax import lax
from jax.experimental import pallas as pl
from jax.experimental.pallas import tpu as pltpu
from jax.sharding import PartitionSpec as P

GROUPS = 4
SPAN = 16
TOP_K = 2
CORES = 2
SIDE = 2
LANES = 128
EPS = 1e-06
MESH = pl.DeviceIdType.MESH
KINDS = 14
X, Y, DX, DY, XP, YP, FX, FY, FDX, FDY, GX, GY, GDX, GDY = range(KINDS)

def from_behind(value, axis, steps):
    count = lax.axis_size(axis)
    first, last = (max(0, -steps), min(count, count - steps))
    return lax.ppermute(value, axis, [(source, source + steps) for source in range(first, last)])


def rms_scale(values, gain):
    return values * lax.rsqrt(jnp.mean(values * values, axis=-1, keepdims=True) + EPS) * gain


def slot_table(chosen_ids, experts, capacity):
    flat_ids = chosen_ids.reshape(-1)
    matches = (flat_ids[:, None] == jnp.arange(experts, dtype=jnp.int32)[None, :]).astype(jnp.int32)
    before = jnp.cumsum(matches, axis=0) - matches
    slot_of = jnp.sum(before * matches, axis=1)
    target = flat_ids * capacity + slot_of
    return (target[:, None] == jnp.arange(experts * capacity, dtype=jnp.int32)[None, :]).astype(
        jnp.float32
    )


def shards_any(
    residual_in,
    mix_gain,
    pool_weight,
    pool_scale,
    ffn_gain,
    route_ids,
    route_weights,
    gate_weight,
    up_weight,
    down_weight,
):
    tp_count = lax.axis_size("tp")
    sp_count = lax.axis_size("sp")
    tp_index = lax.axis_index("tp")
    tok_count, width = residual_in.shape
    group_width = width // GROUPS
    col_count = pool_weight.shape[1]
    row_count = tok_count // tp_count
    capacity = 2 * TOP_K * row_count // sp_count
    group_index = tp_index * col_count // group_width
    window = jnp.power(2, group_index + 1)
    stream = residual_in.astype(jnp.float32)
    inverse = lax.rsqrt(jnp.mean(stream * stream, axis=-1, keepdims=True) + EPS)
    stream_group = lax.dynamic_slice_in_dim(stream, group_index * group_width, group_width, 1)
    gain_group = lax.dynamic_slice_in_dim(mix_gain, group_index * group_width, group_width, 0)
    normed_group = (stream_group * inverse * gain_group).astype(jnp.bfloat16)
    rim_rows = from_behind(normed_group[tok_count - SPAN :], "sp", 1)
    extended = jnp.concatenate([rim_rows, normed_group], axis=0).astype(jnp.float32)
    window_sum = jnp.zeros((tok_count, group_width), jnp.float32)
    for offset in range(SPAN):
        window_sum = window_sum + jnp.where(
            offset < window, extended[SPAN - offset : SPAN - offset + tok_count], 0.0
        )
    position = lax.axis_index("sp") * tok_count + jnp.arange(tok_count, dtype=jnp.int32)
    divisor = jnp.minimum(position + 1, window).astype(jnp.float32)
    pooled = (window_sum / divisor[:, None] - extended[SPAN:]).astype(jnp.bfloat16)
    mixed = (jnp.dot(pooled, pool_weight, preferred_element_type=jnp.float32) * pool_scale).astype(
        jnp.bfloat16
    )
    stream_own = lax.dynamic_slice_in_dim(stream, tp_index * row_count, row_count, 0)
    mixed_own = lax.all_to_all(mixed, "tp", split_axis=0, concat_axis=1, tiled=True)
    after_own = (stream_own + mixed_own.astype(jnp.float32)).astype(jnp.bfloat16)
    normed_own = rms_scale(after_own.astype(jnp.float32), ffn_gain).astype(jnp.bfloat16)
    ids_own = lax.dynamic_slice_in_dim(route_ids, tp_index * row_count, row_count, 0)
    table_own = slot_table(ids_own, sp_count, capacity)
    repeated = jnp.repeat(normed_own, TOP_K, axis=0)
    outgoing = lax.dot_general(
        table_own.astype(jnp.bfloat16),
        repeated,
        (((0,), (0,)), ((), ())),
        preferred_element_type=jnp.float32,
    )
    outgoing = outgoing.astype(jnp.bfloat16).reshape(sp_count, capacity, width)
    arrived = lax.all_to_all(outgoing, "sp", split_axis=0, concat_axis=0, tiled=True)
    piece = lax.all_gather(arrived, "tp", axis=0, tiled=True)
    flat_rows = piece.reshape(-1, width)
    gate_part = jnp.dot(flat_rows, gate_weight[0], preferred_element_type=jnp.float32)
    up_part = jnp.dot(flat_rows, up_weight[0], preferred_element_type=jnp.float32)
    hidden = (jax.nn.silu(gate_part) * up_part).astype(jnp.bfloat16)
    hidden_all = hidden.reshape(piece.shape[0], piece.shape[1], hidden.shape[1])
    hidden_flat = hidden_all.reshape(-1, hidden_all.shape[-1])
    term = jnp.dot(hidden_flat, down_weight[0], preferred_element_type=jnp.float32)
    summed = lax.psum_scatter(
        term.astype(jnp.bfloat16).astype(jnp.float32).astype(jnp.bfloat16),
        "tp",
        scatter_dimension=0,
        tiled=True,
    )
    expert_out = summed.reshape(sp_count, capacity, width)
    returned_rows = lax.all_to_all(expert_out, "sp", split_axis=0, concat_axis=0, tiled=True)
    weights_own = lax.dynamic_slice_in_dim(route_weights, tp_index * row_count, row_count, 0)
    weight_table = jnp.einsum(
        "rk,rkc->rc", weights_own, table_own.reshape(row_count, TOP_K, sp_count * capacity)
    )
    expert_mix = jnp.dot(
        weight_table,
        returned_rows.reshape(-1, width).astype(jnp.float32),
        precision=lax.Precision.HIGHEST,
    )
    out_own = (after_own.astype(jnp.float32) + expert_mix).astype(jnp.bfloat16)
    return lax.all_gather(out_own, "tp", axis=0, tiled=True)


class Place:
    def __init__(self, send_sem, recv_sem):
        self.sp, self.tp = lax.axis_index("sp"), lax.axis_index("tp")
        self.levels = lax.axis_size("sp") // CORES
        self.z, self.c = self.sp // CORES, self.sp % CORES
        y, x = self.tp // SIDE, self.tp % SIDE
        self.tx = y * SIDE + (1 - x)
        self.ty = (1 - y) * SIDE + x
        self.td = (1 - y) * SIDE + (1 - x)
        self.send_sem, self.recv_sem = send_sem, recv_sem
        partner = self.z * CORES + (1 - self.c)
        self.partner = (partner, self.tp)
        along_x, along_y = (self.sp, self.tx), (self.sp, self.ty)
        self.to = {kind: along_x for kind in (X, XP, DX, FX, FDX, GX, GDX)}
        self.to.update({kind: along_y for kind in (Y, YP, DY, FY, FDY, GY, GDY)})

    def copy(self, kind, index, src, dst):
        return pltpu.make_async_remote_copy(
            src_ref=src,
            dst_ref=dst,
            send_sem=self.send_sem.at[kind, index],
            recv_sem=self.recv_sem.at[kind, index],
            device_id=self.to[kind],
            device_id_type=MESH,
        )

    def offsets(self):
        order = [0]
        for distance in range(1, self.levels):
            order += [-distance, distance]
        return order


def greet(place):
    barrier = pltpu.get_barrier_semaphore()

    def hello(target):
        pl.semaphore_signal(barrier, inc=1, device_id=target, device_id_type=MESH)

    count = lax.axis_size("sp")
    hello(place.to[X])
    hello(place.to[Y])
    for step in range(1, count):
        hello((lax.rem(place.sp + step, count), place.tp))
    pl.semaphore_wait(barrier, count + 1)


def level_order(place):
    everywhere = range(place.levels)
    orders = []
    for z in everywhere:
        offsets = [offset for offset in place.offsets() if 0 <= z + offset < place.levels]
        orders.append([z + offset for offset in offsets])
    steps = []
    for index in everywhere:
        level = jnp.int32(orders[0][index])
        for z in everywhere[1:]:
            level = jnp.where(place.z == z, orders[z][index], level)
        steps.append(level)
    return steps


PLAN = [
    ("spread_line", 0), ("relay", 2), ("relay", 1), ("spread_diagonal", 0), ("spread_line", 1),
    ("spread_last", 0), ("pick", 0), ("grow", 0), ("spread_line", 2), ("shrink", 0),
    ("spread_diagonal", 1), ("relay", 3), ("relay_diagonal", 1), ("spread_last", 1), ("first", 0),
    ("pick", 1), ("relay_diagonal", 2), ("grow", 1), ("shrink", 1), ("spread_line", 3),
    ("spread_diagonal", 2), ("first", 1), ("spread_last", 2), ("relay_diagonal", 3), ("pick", 2),
    ("grow", 2), ("shrink", 2), ("spread_diagonal", 3), ("spread_last", 3), ("first", 2),
    ("pick", 3), ("grow", 3), ("shrink", 3), ("second", 2), ("first", 3), ("third", 2),
    ("second", 3), ("third", 3), ("second", 1), ("second", 0), ("third", 1), ("finish", 0),
]


def schedule(levels):
    if levels == 1 + max(step for _, step in PLAN):
        return PLAN
    plan = []
    for turn in range(levels + 3):
        step = turn - 2
        plan += [("relay", turn), ("relay_diagonal", step)]
        plan += [("spread_line", turn), ("spread_diagonal", turn - 1), ("spread_last", step)]
        plan += [("pick", step), ("first", step - 1), ("grow", step), ("second", step - 2)]
        plan += [("shrink", step), ("third", step - 3)]
    plan += [("second", levels - 1), ("third", levels - 2), ("third", levels - 1), ("finish", 0)]
    return [(stage, step) for stage, step in plan if 0 <= step < levels]


def layer_kernel(
    own_ref, meta_ref, gain_ref, gate_ref, up_ref, down_ref, out_ref,
    held, metas, slot_rows, weight_rows, gu, dn, picked, hid, spread, scale, parts,
    r_pair, s_diag, r_ydiag, r_xdiag, s_x, s_y, r_x, r_y, s_z, r_z,
    send_sem, recv_sem, g_send, g_recv, p_send, p_recv, z_send, z_recv, m_send, m_recv,
    w_sem, l_sem,
):
    place = Place(send_sem, recv_sem)
    rows, cols = own_ref.shape
    width = held.shape[2]
    slots = spread.shape[2]
    sp_count, tiles = lax.axis_size("sp"), SIDE * SIDE
    half = rows // 2
    z, c, tp = place.z, place.c, place.tp
    chunk, wide = 32, 256
    pieces, _, pair_lanes = gu.shape
    lanes_each = pair_lanes // 2
    order = level_order(place)

    def gate_copy(piece, side):
        source = (gate_ref, up_ref)[side]
        return pltpu.make_async_copy(
            source.at[0, :, pl.ds(piece * lanes_each, lanes_each)],
            gu.at[piece, :, pl.ds(side * lanes_each, lanes_each)],
            w_sem.at[piece, side],
        )

    down_copy = pltpu.make_async_copy(down_ref.at[0], dn, w_sem.at[pieces, 0])

    def block(level, core, tile, first=0, count=rows):
        at = pl.ds(pl.multiple_of(core * rows + first, half), count)
        return held.at[level, at, pl.ds(pl.multiple_of(tile * cols, cols), cols)]

    def meta_copy(step):
        return pltpu.make_async_remote_copy(
            src_ref=meta_ref,
            dst_ref=metas.at[place.sp],
            send_sem=m_send.at[step],
            recv_sem=m_recv.at[step],
            device_id=(lax.rem(place.sp + step, sp_count), tp),
            device_id_type=MESH,
        )

    middle = (z > 0) & (z < place.levels - 1)
    has_up, has_down = z < place.levels - 1, z > 0

    def line(level, diagonal, up=True):
        ref = block(level, c, place.td if diagonal else tp)
        return pltpu.make_async_remote_copy(
            src_ref=ref,
            dst_ref=ref,
            send_sem=z_send.at[2 * diagonal + up, level],
            recv_sem=z_recv.at[diagonal, level],
            device_id=((z + 1 if up else z - 1) * CORES + c, tp),
            device_id_type=MESH,
        )

    def line_own(diagonal, act):
        pl.when(has_up)(lambda: act(line(z, diagonal, True)))
        pl.when(has_down)(lambda: act(line(z, diagonal, False)))

    def line_on(level, diagonal, act):
        pl.when(middle & (level < z))(lambda: act(line(level, diagonal, True)))
        pl.when(middle & (level > z))(lambda: act(line(level, diagonal, False)))

    def line_relay(step, diagonal):
        level = order[step]
        if step:
            pl.when(middle)(lambda: line(level, diagonal).wait_recv())
            line_on(level, diagonal, lambda copy: copy.start())

    def line_end(level, diagonal):
        pl.when(jnp.logical_not(middle))(lambda: line(level, diagonal).wait_recv())

    def core_copy(level, tile, core):
        ref = block(level, core, tile)
        return pltpu.make_async_remote_copy(
            src_ref=ref,
            dst_ref=ref,
            send_sem=g_send.at[level, tile],
            recv_sem=g_recv.at[level, tile],
            device_id=place.partner,
            device_id_type=MESH,
        )

    def whole(kind, level, tile):
        ref = block(level, c, tile)
        return place.copy(kind, level, ref, ref)

    def part(kind, level, tile):
        ref = block(level, c, tile, 0 if kind == GDY else half, half)
        return place.copy(kind, level, ref, ref)

    def spread_line(step):
        level = order[step]
        if step:
            line_end(level, 0)
        whole(GX, level, tp).start()
        whole(GY, level, tp).start()
        core_copy(level, tp, c).start()

    def spread_diagonal(step):
        level = order[step]
        whole(GX, level, place.tx).wait_recv()
        if step == 0:
            part(GDY, level, place.tx).start()
        core_copy(level, place.tx, c).start()
        whole(GY, level, place.ty).wait_recv()
        if step == 0:
            part(GDX, level, place.ty).start()
        core_copy(level, place.ty, c).start()

    def spread_last(step):
        level = order[step]
        if step:
            line_end(level, 1)
        else:
            part(GDY, level, place.td).wait_recv()
            part(GDX, level, place.td).wait_recv()
            line_own(1, lambda copy: copy.start())
        core_copy(level, place.td, c).start()

    def number_slots():
        for hop in range(1, sp_count):
            meta_copy(hop).wait_recv()
        expert = place.sp.astype(jnp.float32)
        match = jnp.zeros((sp_count, rows), jnp.float32)
        weight = jnp.zeros((sp_count, rows), jnp.float32)
        for k in range(TOP_K):
            named = jnp.where(metas[:, k] == expert, 1.0, 0.0)
            match = match + named
            weight = weight + named * metas[:, TOP_K + k]
        block_rows = rows // tiles
        source = lax.broadcasted_iota(jnp.int32, (rows, rows), 0)
        target = lax.broadcasted_iota(jnp.int32, (rows, rows), 1)
        earlier = (source < target) & (source // block_rows == target // block_rows)
        earlier = jnp.where(earlier, 1.0, 0.0).astype(jnp.bfloat16)
        before = jnp.dot(match.astype(jnp.bfloat16), earlier, preferred_element_type=jnp.float32)
        at = lax.broadcasted_iota(jnp.int32, (sp_count, rows), 1)
        base = (at // block_rows * (slots // tiles)).astype(jnp.float32)
        slot_rows[...] = jnp.where(match > 0, before + base, -1.0)
        weight_rows[...] = weight

    def pick(step):
        level = order[step]
        if step == 0:
            number_slots()
        for tile in range(tiles):
            core_copy(level, tile, 1 - c).wait_recv()
        for b in range(CORES):
            source = pl.ds(level * CORES + b, 1)
            at = lax.broadcasted_iota(jnp.int32, (slots, rows), 0).astype(jnp.float32)
            chosen = at == slot_rows[source]
            table = jnp.where(chosen, 1.0, 0.0)
            scale[b] = jnp.sum(jnp.where(chosen, weight_rows[source], 0.0), axis=1, keepdims=True)
            spread[b] = table.T.astype(jnp.bfloat16)
            table = table.astype(jnp.bfloat16)
            squares = jnp.zeros((slots, 1), jnp.float32)
            into = slice(b * slots, (b + 1) * slots)
            for start in range(0, width, wide):
                lanes = slice(start, start + wide)
                value = jnp.dot(
                    table,
                    held[level, b * rows : (b + 1) * rows, lanes],
                    preferred_element_type=jnp.float32,
                )
                squares = squares + jnp.sum(value * value, axis=1, keepdims=True)
                picked[into, lanes] = value.astype(jnp.bfloat16)
            inverse = lax.rsqrt(squares / width + EPS)
            for start in range(0, width, wide):
                lanes = slice(start, start + wide)
                value = picked[into, lanes].astype(jnp.float32) * inverse * gain_ref[:, lanes]
                picked[into, lanes] = value.astype(jnp.bfloat16)

    def grow(step):
        for piece in range(pieces):
            if step == 0:
                gate_copy(piece, 0).wait()
                gate_copy(piece, 1).wait()
            both = jnp.dot(picked[...], gu[piece], preferred_element_type=jnp.float32)
            gate, up = both[:, :lanes_each], both[:, lanes_each:]
            lanes = slice(piece * lanes_each, (piece + 1) * lanes_each)
            hid[:, lanes] = (jax.nn.silu(gate) * up).astype(jnp.bfloat16)

    def pair_copy(level, tile):
        lanes = pl.ds(pl.multiple_of(tile * cols, cols), cols)
        return pltpu.make_async_remote_copy(
            src_ref=parts.at[level, 1 - c, :, lanes],
            dst_ref=r_pair.at[level, :, lanes],
            send_sem=p_send.at[level, tile],
            recv_sem=p_recv.at[level, tile],
            device_id=place.partner,
            device_id_type=MESH,
        )

    def shrink(step):
        level = order[step]
        if step == 0:
            down_copy.wait()
        for tile in (place.td, place.tx, place.ty, tp):
            lanes = pl.ds(pl.multiple_of(tile * cols, cols), cols)
            term = jnp.dot(hid[...], dn[:, lanes], preferred_element_type=jnp.float32)
            for b in range(CORES):
                scaled = (term[b * slots : (b + 1) * slots] * scale[b]).astype(jnp.bfloat16)
                value = jnp.dot(spread[b], scaled, preferred_element_type=jnp.float32)
                parts[level, b, :, lanes] = value.astype(jnp.bfloat16)
            pair_copy(level, tile).start()

    def summed(level, tile, row, count=chunk):
        at = pl.ds(pl.multiple_of(row, chunk), count)
        lanes = pl.ds(pl.multiple_of(tile * cols, cols), cols)
        mine = parts[level, c, at, lanes].astype(jnp.float32)
        return mine + r_pair[level, at, lanes].astype(jnp.float32)

    def over(first, last, body):
        def step(index, carry):
            body(pl.multiple_of(first + index * chunk, chunk))
            return carry

        lax.fori_loop(0, (last - first) // chunk, step, 0)

    def diag(kind, level):
        if kind == DY:
            return place.copy(kind, level, s_diag.at[level, pl.ds(0, half)], r_ydiag.at[level])
        return place.copy(kind, level, s_diag.at[level, pl.ds(half, half)], r_xdiag.at[level])

    def side(kind, level):
        source, arrived = (s_x, r_x) if kind in (X, XP) else (s_y, r_y)
        at = pl.ds(0 if kind in (X, YP) else half, half)
        return place.copy(kind, level, source.at[level, at], arrived.at[level, at])

    def owner_copy(level, part_of, arriving):
        at = pl.ds(part_of * half, half)
        return pltpu.make_async_remote_copy(
            src_ref=s_z.at[level, at],
            dst_ref=r_z.at[level if arriving else z, at],
            send_sem=z_send.at[4 + part_of, level],
            recv_sem=z_recv.at[2 + part_of, level if arriving else z],
            device_id=(level * CORES + c, tp),
            device_id_type=MESH,
        )

    def first(step):
        level = order[step]

        def plain(buffer, tile):
            def body(row):
                buffer[level, pl.ds(row, chunk)] = summed(level, tile, row).astype(jnp.bfloat16)

            return body

        pair_copy(level, place.td).wait_recv()
        over(0, half, plain(s_diag, place.td))
        diag(DY, level).start()
        over(half, rows, plain(s_diag, place.td))
        diag(DX, level).start()
        pair_copy(level, place.tx).wait_recv()
        over(half, rows, plain(s_x, place.tx))
        side(XP, level).start()
        pair_copy(level, place.ty).wait_recv()
        over(0, half, plain(s_y, place.ty))
        side(YP, level).start()

    def second(step):
        level = order[step]

        def joined(buffer, tile, arrived, base):
            def body(row):
                other = arrived[level, pl.ds(pl.multiple_of(row - base, chunk), chunk)]
                total = summed(level, tile, row) + other.astype(jnp.float32)
                buffer[level, pl.ds(row, chunk)] = total.astype(jnp.bfloat16)

            return body

        diag(DY, level).wait_recv()
        over(0, half, joined(s_x, place.tx, r_ydiag, 0))
        side(X, level).start()
        diag(DX, level).wait_recv()
        over(half, rows, joined(s_y, place.ty, r_xdiag, half))
        side(Y, level).start()

    def plane_sum(level, row):
        at = pl.ds(row, chunk)
        total = summed(level, tp, row)
        return total + r_x[level, at].astype(jnp.float32) + r_y[level, at].astype(jnp.float32)

    def plane_wait(level, part_of):
        if part_of == 0:
            pair_copy(level, tp).wait_recv()
        for kind in ((X, YP), (XP, Y))[part_of]:
            side(kind, level).wait_recv()

    def third(step):
        if step == 0:
            return
        level = order[step]

        def body(row):
            s_z[level, pl.ds(row, chunk)] = plane_sum(level, row).astype(jnp.bfloat16)

        for part_of in range(2):
            plane_wait(level, part_of)
            over(part_of * half, (part_of + 1) * half, body)
            owner_copy(level, part_of, False).start()

    def final(kind, tile, part_of):
        at = pl.ds(part_of * half, half)
        ref = out_ref.at[at, pl.ds(pl.multiple_of(tile * cols, cols), cols)]
        return place.copy(kind, part_of, ref, ref)

    def finish(step):
        level = order[step]

        def body(row):
            at = pl.ds(row, chunk)
            total = plane_sum(level, row)
            for other in order[1:]:
                total = total + r_z[other, at].astype(jnp.float32)
            total = total + own_ref[at].astype(jnp.float32)
            lanes = pl.ds(pl.multiple_of(tp * cols, cols), cols)
            out_ref[at, lanes] = total.astype(jnp.bfloat16)

        for part_of in range(2):
            plane_wait(level, part_of)
            for other in order[1:]:
                owner_copy(other, part_of, True).wait_recv()
            over(part_of * half, (part_of + 1) * half, body)
            final(FX, tp, part_of).start()
            final(FY, tp, part_of).start()

    local = pltpu.make_async_copy(own_ref, block(z, c, tp), l_sem.at[0])
    local.start()
    local_meta = pltpu.make_async_copy(meta_ref, metas.at[place.sp], l_sem.at[1])
    local_meta.start()
    for piece in range(pieces):
        gate_copy(piece, 0).start()
        gate_copy(piece, 1).start()
    down_copy.start()
    local.wait()
    local_meta.wait()
    greet(place)
    for hop in range(1, sp_count):
        meta_copy(hop).start()
    line_own(0, lambda copy: copy.start())

    stages = {
        "relay": lambda step: line_relay(step, 0),
        "relay_diagonal": lambda step: line_relay(step, 1),
        "spread_line": spread_line,
        "spread_diagonal": spread_diagonal,
        "spread_last": spread_last,
        "pick": pick,
        "grow": grow,
        "shrink": shrink,
        "first": first,
        "second": second,
        "third": third,
        "finish": finish,
    }
    for stage, step in schedule(place.levels):
        stages[stage](step)

    final(FX, place.tx, 0).wait_recv()
    final(FDY, place.tx, 0).start()
    final(FY, place.ty, 0).wait_recv()
    final(FY, place.ty, 1).wait_recv()
    final(FDX, place.ty, 1).start()
    final(FX, place.tx, 1).wait_recv()
    for hop in range(1, sp_count):
        meta_copy(hop).wait_send()
    line_own(0, lambda copy: copy.wait_send())
    line_own(1, lambda copy: copy.wait_send())
    for step, level in enumerate(order):
        whole(GX, level, tp).wait_send()
        whole(GY, level, tp).wait_send()
        for tile in range(tiles):
            core_copy(level, tile, c).wait_send()
            pair_copy(level, tile).wait_send()
        for kind in (DX, DY):
            diag(kind, level).wait_send()
        for kind in (X, Y, XP, YP):
            side(kind, level).wait_send()
        if step:
            for part_of in range(2):
                line_on(level, part_of, lambda copy: copy.wait_send())
                owner_copy(level, part_of, False).wait_send()
        else:
            part(GDY, level, place.tx).wait_send()
            part(GDX, level, place.ty).wait_send()
    final(FDY, place.td, 0).wait_recv()
    final(FDX, place.td, 1).wait_recv()
    for part_of in range(2):
        final(FX, tp, part_of).wait_send()
        final(FY, tp, part_of).wait_send()
    final(FDY, place.tx, 0).wait_send()
    final(FDX, place.ty, 1).wait_send()


def layer_all(own, meta, gain, gate, up, down, capacity, sp_count, tp_count):
    rows, cols = own.shape
    width = tp_count * cols
    hidden = gate.shape[2]
    levels = sp_count // CORES
    slots = capacity * tp_count
    vmem = pl.BlockSpec(memory_space=pltpu.VMEM)
    hbm = pl.BlockSpec(memory_space=pl.ANY)
    whole = pltpu.VMEM((levels, rows, cols), jnp.bfloat16)
    halved = pltpu.VMEM((levels, rows // 2, cols), jnp.bfloat16)
    pieces = hidden // LANES
    return pl.pallas_call(
        layer_kernel,
        out_shape=jax.ShapeDtypeStruct((rows, width), own.dtype),
        in_specs=[vmem, vmem, vmem, hbm, hbm, hbm],
        out_specs=vmem,
        scratch_shapes=[
            pltpu.VMEM((levels, CORES * rows, width), jnp.bfloat16),
            pltpu.VMEM((sp_count,) + meta.shape, jnp.float32),
            pltpu.VMEM((sp_count, rows), jnp.float32),
            pltpu.VMEM((sp_count, rows), jnp.float32),
            pltpu.VMEM((pieces, width, 2 * LANES), jnp.bfloat16),
            pltpu.VMEM((hidden, width), jnp.bfloat16),
            pltpu.VMEM((CORES * slots, width), jnp.bfloat16),
            pltpu.VMEM((CORES * slots, hidden), jnp.bfloat16),
            pltpu.VMEM((CORES, rows, slots), jnp.bfloat16),
            pltpu.VMEM((CORES, slots, 1), jnp.float32),
            pltpu.VMEM((levels, CORES, rows, width), jnp.bfloat16),
            pltpu.VMEM((levels, rows, width), jnp.bfloat16),
            whole, halved, halved, whole, whole, whole, whole, whole, whole,
            pltpu.SemaphoreType.DMA((KINDS, max(2, levels))),
            pltpu.SemaphoreType.DMA((KINDS, max(2, levels))),
            pltpu.SemaphoreType.DMA((levels, tp_count)),
            pltpu.SemaphoreType.DMA((levels, tp_count)),
            pltpu.SemaphoreType.DMA((levels, tp_count)),
            pltpu.SemaphoreType.DMA((levels, tp_count)),
            pltpu.SemaphoreType.DMA((6, levels)),
            pltpu.SemaphoreType.DMA((4, levels)),
            pltpu.SemaphoreType.DMA((sp_count,)),
            pltpu.SemaphoreType.DMA((sp_count,)),
            pltpu.SemaphoreType.DMA((pieces + 1, 2)),
            pltpu.SemaphoreType.DMA((2,)),
        ],
        compiler_params=pltpu.CompilerParams(
            collective_id=0, has_side_effects=True, vmem_limit_bytes=62 * 1024 * 1024
        ),
        name="layer_all",
    )(own, meta, gain, gate, up, down)


def shards(
    residual_in,
    mix_gain,
    pool_weight,
    pool_scale,
    ffn_gain,
    route_ids,
    route_weights,
    gate_weight,
    up_weight,
    down_weight,
):
    tp_count = lax.axis_size("tp")
    sp_count = lax.axis_size("sp")
    tp_index = lax.axis_index("tp")
    tok_count, width = residual_in.shape
    group_width = width // GROUPS
    col_count = pool_weight.shape[1]
    block_rows = tok_count // tp_count
    capacity = 2 * TOP_K * block_rows // sp_count
    group_index = tp_index * col_count // group_width
    window = jnp.power(2, group_index + 1)
    stream = residual_in.astype(jnp.float32)
    inverse = lax.rsqrt(jnp.mean(stream * stream, axis=-1, keepdims=True) + EPS)
    stream_group = lax.dynamic_slice_in_dim(residual_in, group_index * group_width, group_width, 1)
    stream_group = stream_group.astype(jnp.float32)
    gain_group = lax.dynamic_slice_in_dim(mix_gain, group_index * group_width, group_width, 0)
    normed_group = (stream_group * inverse * gain_group).astype(jnp.bfloat16)
    rim_rows = from_behind(normed_group[tok_count - SPAN :], "sp", 1)
    extended = jnp.concatenate([rim_rows, normed_group], axis=0).astype(jnp.float32)
    window_sum = jnp.zeros((tok_count, group_width), jnp.float32)
    for offset in range(SPAN):
        window_sum = window_sum + jnp.where(
            offset < window, extended[SPAN - offset : SPAN - offset + tok_count], 0.0
        )
    position = lax.axis_index("sp") * tok_count + jnp.arange(tok_count, dtype=jnp.int32)
    divisor = jnp.minimum(position + 1, window).astype(jnp.float32)
    pooled = (window_sum / divisor[:, None] - extended[SPAN:]).astype(jnp.bfloat16)
    mixed = (jnp.dot(pooled, pool_weight, preferred_element_type=jnp.float32) * pool_scale).astype(
        jnp.bfloat16
    )
    stream_own = lax.dynamic_slice_in_dim(residual_in, tp_index * col_count, col_count, 1)
    after_own = (stream_own.astype(jnp.float32) + mixed.astype(jnp.float32)).astype(jnp.bfloat16)

    meta = jnp.concatenate(
        [
            route_ids.astype(jnp.float32).T,
            route_weights.T,
            jnp.zeros((8 - 2 * TOP_K, tok_count), jnp.float32),
        ],
        axis=0,
    )
    return layer_all(
        after_own,
        meta,
        ffn_gain[None],
        gate_weight,
        up_weight,
        down_weight,
        capacity,
        sp_count,
        tp_count,
    )


def solution(mesh):
    placed = (
        P("sp", None),
        P(),
        P(None, "tp"),
        P("tp"),
        P(),
        P("sp", None),
        P("sp", None),
        P("sp", None, "tp"),
        P("sp", None, "tp"),
        P("sp", "tp", None),
    )
    square = mesh.shape["tp"] == SIDE * SIDE and mesh.shape["sp"] % CORES == 0
    return jax.shard_map(
        shards if square else shards_any,
        mesh=mesh,
        in_specs=placed,
        out_specs=P("sp", None),
        check_vma=False,
    )
```

time: 140 us -> 115 us (0.82)
  the two profiles are of different devices: /device:TPU:18 before, /device:TPU:0 now
where the time goes in v2:
time: 115 us
  Pallas kernels  102 us (89%)
  other arithmetic  4.74 us (4%)
  local copies, waits for them, and re-layouts  3.15 us (3%)
  matrix products  2.97 us (3%)
  starting transfers between devices  2.4 us (2%)
    pallas_call x1, Pallas kernels, layer_all(): pl.pallas_call(layer_kernel, out_shape=jax.ShapeDtypeStruct((rows, width)...  102 us
    dot_general x1, matrix products, shards(): jnp.dot(pooled, pool_weight, preferred_element_type=jnp.float32)  2.97 us
    ppermute x1, starting transfers between devices, from_behind(): lax.ppermute(value, axis, [(source, source + steps) for source in range(f...  2.4 us
    unnamed x3, local copies, waits for them, and re-layouts  2.31 us
  transfers between devices with their start and end apart: 1, of which 0 were waited for; matrix products, arithmetic and copies ran while one was open for 2% of the time, Pallas kernels for 0%

profile of v2, /device:TPU:0, one launch (start us, length us, event | category | flops | bytes accessed | tf_op | source)
XLA Modules:
  0.0 115.1 jit_solution(8428747848781366213)
XLA Ops:
  0.0 0.0 copy-start
  0.0 1.6 %multiply_reduce_fusion = f32[256]{0:T(256)S(1)} fusion(bf16[256,2048]{1,0:T(8,128)(2,1)} %param.10), kind=kLoop, calls=%fused_computation | loop fusion | flops 1572608 | bytes 1049600 | tf_op jit(solution)/shard_map/reduce_sum | solution.py:683
  1.6 0.8 dynamic_slice.11
  2.4 1.1 multiply_convert_fusion
  3.4 2.4 %collective-permute-start = (bf16[16,512]{1,0:T(8,128)(2,1)S(1)}, bf16[16,512]{1,0:T(8,128)(2,1)S(1)}, u32[]{:S(2)}, u32[]{:S(2)}) collective-permute-start(bf16[16,512]{1,0:T(8,128)(2,1)S(1)} %slice.69), channel_id=1, source_target_pairs={{0,4},{4,8},{8,12},{12,16},{16,20},{20,24},{24,28},{1,5},{5,9},{9,... | collective-permute-start | bytes 49160 | tf_op jit(solution)/shard_map/ppermute | solution.py:22
  5.9 0.7 convert_bitcast_fusion
  6.6 0.1 pad.2.clone
  6.6 1.3 %maximum_maximum_fusion.meta_ref = f32[8,256]{1,0:T(8,128)} fusion(f32[2,256]{1,0:T(2,128)} %bitcast.6, f32[2,256]{1,0:T(2,128)S(1)} %convert_bitcast_fusion, f32[8]{0:T(128)S(1)} %pad.2.clone), kind=kLoop, calls=%fused_computation.41 | loop fusion | flops 4096 | bytes 12320 | tf_op jit(solution)/shard_map/concatenate | solution.py:704
  8.0 0.0 collective-permute-done
  8.0 0.1 maximum_convert_fusion
  8.1 0.0 copy-done
  8.1 3.0 %fusion.3.own_ref = bf16[256,512]{1,0:T(8,128)(2,1)} fusion(bf16[512,512]{1,0:T(8,128)(2,1)S(1)} %copy-done, f32[512]{0:T(512)} %param.13, bf16[256,2048]{1,0:T(8,128)(2,1)} %param.10, s32[]{:T(128)S(6)} %select_n.130, f32[272,512]{1,0:T(8,128)S(1)} %maximum_convert_fusion, f32[256]{0:T(256)S(1)} %minimum_convert_fusion, pred[]{:T(512)S(6)} %gt.63, ...), kind=kOutput, calls=%fused_computation.5 | convolution fusion | flops 139460608 | bytes 9440276 | tf_op jit(solution)/shard_map/dot_general | solution.py:698
  11.0 101.7 %layer_all.1 = bf16[256,2048]{1,0:T(8,128)(2,1)} custom-call(bf16[256,512]{1,0:T(8,128)(2,1)} %fusion.3.own_ref, f32[8,256]{1,0:T(8,128)} %maximum_maximum_fusion.meta_ref, f32[1,2048]{1,0:T(1,128)} %bitcast.5, bf16[1,2048,896]{2,1,0:T(8,128)(2,1)} %gate_ref.1, bf16[1,2048,896]{2,1,0:T(8,128)(2,1)} %up_ref.1, bf16[1,896,2048]{2,1,0:T(8,128)(2,1)} %down_ref.1), custom_call_target="tpu_custom_call" | custom-call | tf_op jit(solution)/shard_map/layer_all/pallas_call | solution.py:621
  112.8 2.3 %copy.12 = bf16[256,2048]{1,0:T(8,128)(2,1)} copy(bf16[256,2048]{1,0:T(8,128)(2,1)} %layer_all.1) | data formatting | bytes 2097152
  (4 shorter events, 0.0 us)
Async XLA Ops:
  0.0 8.1 %copy-start = (bf16[512,512]{1,0:T(8,128)(2,1)S(1)}, bf16[512,512]{1,0:T(8,128)(2,1)}, u32[]{:S(2)}) copy-start(bf16[512,512]{1,0:T(8,128)(2,1)} %param.12) | copy-start | bytes 1572868
  3.4 4.5 %collective-permute-start = (bf16[16,512]{1,0:T(8,128)(2,1)S(1)}, bf16[16,512]{1,0:T(8,128)(2,1)S(1)}, u32[]{:S(2)}, u32[]{:S(2)}) collective-permute-start(bf16[16,512]{1,0:T(8,128)(2,1)S(1)} %slice.69), channel_id=1, source_target_pairs={{0,4},{4,8},{8,12},{12,16},{16,20},{20,24},{24,28},{1,5},{5,9},{9,... | collective-permute-start | bytes 49160 | tf_op jit(solution)/shard_map/ppermute | solution.py:22

commit v3 on v2

--- a/solution.py
+++ b/solution.py
@@ -210,11 +210,12 @@
 
 
 def layer_kernel(
-    own_ref, meta_ref, gain_ref, gate_ref, up_ref, down_ref, out_ref,
-    held, metas, slot_rows, weight_rows, gu, dn, picked, hid, spread, scale, parts,
+    stream_ref, mix_ref, pool_ref, pool_scale_ref, ids_ref, shares_ref,
+    gain_ref, gate_ref, up_ref, down_ref, out_ref,
+    own_ref, extended, rim_out, rim_in, meta_ref, held, metas, slot_rows, weight_rows, gu, dn, picked, hid, spread, scale, parts,
     r_pair, s_diag, r_ydiag, r_xdiag, s_x, s_y, r_x, r_y, s_z, r_z,
     send_sem, recv_sem, g_send, g_recv, p_send, p_recv, z_send, z_recv, m_send, m_recv,
-    w_sem, l_sem,
+    w_sem, l_sem, rim_send, rim_recv,
 ):
     place = Place(send_sem, recv_sem)
     rows, cols = own_ref.shape
@@ -539,19 +540,68 @@
             final(FX, tp, part_of).start()
             final(FY, tp, part_of).start()
 
-    local = pltpu.make_async_copy(own_ref, block(z, c, tp), l_sem.at[0])
-    local.start()
-    local_meta = pltpu.make_async_copy(meta_ref, metas.at[place.sp], l_sem.at[1])
-    local_meta.start()
+    def rim_copy(step):
+        return pltpu.make_async_remote_copy(
+            src_ref=rim_out,
+            dst_ref=rim_in,
+            send_sem=rim_send.at[0],
+            recv_sem=rim_recv.at[0],
+            device_id=(place.sp + step, tp),
+            device_id_type=MESH,
+        )
+
+    mine = pl.ds(pl.multiple_of(tp * cols, cols), cols)
+
+    def normalize():
+        squares = jnp.zeros((rows, 1), jnp.float32)
+        for start in range(0, width, cols):
+            value = stream_ref[:, start : start + cols].astype(jnp.float32)
+            squares = squares + jnp.sum(value * value, axis=1, keepdims=True)
+        inverse = lax.rsqrt(squares / width + EPS)
+        value = stream_ref[:, mine].astype(jnp.float32) * inverse * mix_ref[:, mine]
+        value = value.astype(jnp.bfloat16)
+        extended[SPAN:] = value.astype(jnp.float32)
+        rim_out[...] = value[rows - SPAN :]
+
+    def mix():
+        extended[:SPAN] = rim_in[...].astype(jnp.float32)
+        value = extended[...]
+        sums, reach = value, 1
+        window_sum = jnp.zeros_like(value)
+        for group in range(GROUPS):
+            sums = sums + pltpu.roll(sums, reach, 0)
+            reach = 2 * reach
+            window_sum = jnp.where(tp == group, sums, window_sum)
+        position = place.sp * rows + lax.broadcasted_iota(jnp.int32, (rows, 1), 0)
+        window = 2
+        for group in range(1, GROUPS):
+            window = jnp.where(tp == group, 2 ** (group + 1), window)
+        divisor = jnp.minimum(position + 1, window).astype(jnp.float32)
+        pooled = (window_sum[SPAN:] / divisor - value[SPAN:]).astype(jnp.bfloat16)
+        mixed = jnp.dot(pooled, pool_ref[...], preferred_element_type=jnp.float32)
+        mixed = (mixed * pool_scale_ref[...]).astype(jnp.bfloat16).astype(jnp.float32)
+        after = (stream_ref[:, mine].astype(jnp.float32) + mixed).astype(jnp.bfloat16)
+        own_ref[...] = after
+        held[z, pl.ds(pl.multiple_of(c * rows, rows), rows), mine] = after
+
     for piece in range(pieces):
         gate_copy(piece, 0).start()
         gate_copy(piece, 1).start()
     down_copy.start()
-    local.wait()
+    normalize()
+    meta_ref[...] = jnp.zeros_like(meta_ref)
+    meta_ref[0:TOP_K] = ids_ref[...].astype(jnp.float32)
+    meta_ref[TOP_K : 2 * TOP_K] = shares_ref[...]
+    local_meta = pltpu.make_async_copy(meta_ref, metas.at[place.sp], l_sem.at[0])
+    local_meta.start()
+    pl.when(place.sp == 0)(lambda: rim_in.__setitem__(Ellipsis, jnp.zeros_like(rim_in)))
     local_meta.wait()
     greet(place)
+    pl.when(place.sp < sp_count - 1)(lambda: rim_copy(1).start())
     for hop in range(1, sp_count):
         meta_copy(hop).start()
+    pl.when(place.sp > 0)(lambda: rim_copy(-1).wait_recv())
+    mix()
     line_own(0, lambda copy: copy.start())
 
     stages = {
@@ -579,6 +629,7 @@
     final(FX, place.tx, 1).wait_recv()
     for hop in range(1, sp_count):
         meta_copy(hop).wait_send()
+    pl.when(place.sp < sp_count - 1)(lambda: rim_copy(1).wait_send())
     line_own(0, lambda copy: copy.wait_send())
     line_own(1, lambda copy: copy.wait_send())
     for step, level in enumerate(order):
@@ -607,8 +658,10 @@
     final(FDX, place.ty, 1).wait_send()
 
 
-def layer_all(own, meta, gain, gate, up, down, capacity, sp_count, tp_count):
-    rows, cols = own.shape
+def layer_all(
+    stream, mix_gain, pool, pool_scale, ids, shares, gain, gate, up, down, capacity, sp_count, tp_count
+):
+    rows, cols = stream.shape[0], pool.shape[1]
     width = tp_count * cols
     hidden = gate.shape[2]
     levels = sp_count // CORES
@@ -620,12 +673,17 @@
     pieces = hidden // LANES
     return pl.pallas_call(
         layer_kernel,
-        out_shape=jax.ShapeDtypeStruct((rows, width), own.dtype),
-        in_specs=[vmem, vmem, vmem, hbm, hbm, hbm],
+        out_shape=jax.ShapeDtypeStruct((rows, width), stream.dtype),
+        in_specs=[vmem, vmem, vmem, vmem, vmem, vmem, vmem, hbm, hbm, hbm],
         out_specs=vmem,
         scratch_shapes=[
+            pltpu.VMEM((rows, cols), jnp.bfloat16),
+            pltpu.VMEM((SPAN + rows, cols), jnp.float32),
+            pltpu.VMEM((SPAN, cols), jnp.bfloat16),
+            pltpu.VMEM((SPAN, cols), jnp.bfloat16),
+            pltpu.VMEM((8, rows), jnp.float32),
             pltpu.VMEM((levels, CORES * rows, width), jnp.bfloat16),
-            pltpu.VMEM((sp_count,) + meta.shape, jnp.float32),
+            pltpu.VMEM((sp_count, 8, rows), jnp.float32),
             pltpu.VMEM((sp_count, rows), jnp.float32),
             pltpu.VMEM((sp_count, rows), jnp.float32),
             pltpu.VMEM((pieces, width, 2 * LANES), jnp.bfloat16),
@@ -648,13 +706,15 @@
             pltpu.SemaphoreType.DMA((sp_count,)),
             pltpu.SemaphoreType.DMA((sp_count,)),
             pltpu.SemaphoreType.DMA((pieces + 1, 2)),
-            pltpu.SemaphoreType.DMA((2,)),
+            pltpu.SemaphoreType.DMA((1,)),
+            pltpu.SemaphoreType.DMA((1,)),
+            pltpu.SemaphoreType.DMA((1,)),
         ],
         compiler_params=pltpu.CompilerParams(
             collective_id=0, has_side_effects=True, vmem_limit_bytes=62 * 1024 * 1024
         ),
         name="layer_all",
-    )(own, meta, gain, gate, up, down)
+    )(stream, mix_gain, pool, pool_scale, ids, shares, gain, gate, up, down)
 
 
 def shards(
@@ -671,52 +731,19 @@
 ):
     tp_count = lax.axis_size("tp")
     sp_count = lax.axis_size("sp")
-    tp_index = lax.axis_index("tp")
-    tok_count, width = residual_in.shape
-    group_width = width // GROUPS
-    col_count = pool_weight.shape[1]
-    block_rows = tok_count // tp_count
-    capacity = 2 * TOP_K * block_rows // sp_count
-    group_index = tp_index * col_count // group_width
-    window = jnp.power(2, group_index + 1)
-    stream = residual_in.astype(jnp.float32)
-    inverse = lax.rsqrt(jnp.mean(stream * stream, axis=-1, keepdims=True) + EPS)
-    stream_group = lax.dynamic_slice_in_dim(residual_in, group_index * group_width, group_width, 1)
-    stream_group = stream_group.astype(jnp.float32)
-    gain_group = lax.dynamic_slice_in_dim(mix_gain, group_index * group_width, group_width, 0)
-    normed_group = (stream_group * inverse * gain_group).astype(jnp.bfloat16)
-    rim_rows = from_behind(normed_group[tok_count - SPAN :], "sp", 1)
-    extended = jnp.concatenate([rim_rows, normed_group], axis=0).astype(jnp.float32)
-    window_sum = jnp.zeros((tok_count, group_width), jnp.float32)
-    for offset in range(SPAN):
-        window_sum = window_sum + jnp.where(
-            offset < window, extended[SPAN - offset : SPAN - offset + tok_count], 0.0
-        )
-    position = lax.axis_index("sp") * tok_count + jnp.arange(tok_count, dtype=jnp.int32)
-    divisor = jnp.minimum(position + 1, window).astype(jnp.float32)
-    pooled = (window_sum / divisor[:, None] - extended[SPAN:]).astype(jnp.bfloat16)
-    mixed = (jnp.dot(pooled, pool_weight, preferred_element_type=jnp.float32) * pool_scale).astype(
-        jnp.bfloat16
-    )
-    stream_own = lax.dynamic_slice_in_dim(residual_in, tp_index * col_count, col_count, 1)
-    after_own = (stream_own.astype(jnp.float32) + mixed.astype(jnp.float32)).astype(jnp.bfloat16)
-
-    meta = jnp.concatenate(
-        [
-            route_ids.astype(jnp.float32).T,
-            route_weights.T,
-            jnp.zeros((8 - 2 * TOP_K, tok_count), jnp.float32),
-        ],
-        axis=0,
-    )
+    block_rows = residual_in.shape[0] // tp_count
     return layer_all(
-        after_own,
-        meta,
+        residual_in,
+        mix_gain[None],
+        pool_weight,
+        pool_scale[None],
+        route_ids.T,
+        route_weights.T,
         ffn_gain[None],
         gate_weight,
         up_weight,
         down_weight,
-        capacity,
+        2 * TOP_K * block_rows // sp_count,
         sp_count,
         tp_count,
     )

time: 115 us -> 105 us (0.913)
  other arithmetic: 4.74 us -> 0 us
  matrix products: 2.97 us -> 0 us
  starting transfers between devices: 2.4 us -> 0 us
    dot_general x1 -> x0, matrix products: 2.97 us -> none  [shards(): jnp.dot(pooled, pool_weight, preferred_element_type=jnp.float32)]
    ppermute x1 -> x0, starting transfers between devices: 2.4 us -> none  [from_behind(): lax.ppermute(value, axis, [(source, source + steps) for source in range(f...]
    reduce_sum x1 -> x0, other arithmetic: 1.57 us -> none  [shards(): inverse = lax.rsqrt(jnp.mean(stream * stream, axis=-1, keepdims=True) + EPS)]
    concatenate x1 -> x0, other arithmetic: 1.34 us -> none  [shards(): jnp.concatenate([route_ids.astype(jnp.float32).T, route_weights.T, jnp.ze...]
    unnamed x3 -> x1, local copies, waits for them, and re-layouts: 2.31 us -> 2.3 us
  transfers between devices with their start and end apart: 1 -> 0, of which waited for: 0 -> 0; matrix products, arithmetic and copies ran while one was open for 2% -> 0% of each run, Pallas kernels for 0% -> 0%
where the time goes in v3:
time: 105 us
  Pallas kernels  103 us (98%)
  local copies, waits for them, and re-layouts  2.3 us (2%)
    pallas_call x1, Pallas kernels, layer_all(): pl.pallas_call(layer_kernel, out_shape=jax.ShapeDtypeStruct((rows, width)...  103 us
    unnamed x1, local copies, waits for them, and re-layouts  2.3 us

profile of v3, /device:TPU:0, one launch (start us, length us, event | category | flops | bytes accessed | tf_op | source)
XLA Modules:
  0.0 104.9 jit_solution(16405924169497344636)
XLA Ops:
  0.0 102.6 %layer_all.1 = bf16[256,2048]{1,0:T(8,128)(2,1)} custom-call(bf16[256,2048]{1,0:T(8,128)(2,1)} %stream_ref.1, f32[1,2048]{1,0:T(1,128)} %bitcast.5, bf16[512,512]{1,0:T(8,128)(2,1)} %pool_ref.1, f32[1,512]{1,0:T(1,128)} %bitcast.7, s32[2,256]{1,0:T(2,128)} %bitcast.8, f32[2,256]{1,0:T(2,128)} %bitcast.9, f32[1,2048]{1,0:T(1,128)} %bitcast.6, ...), custom_call_target="tpu_custom_call" | custom-call | tf_op jit(solution)/shard_map/layer_all/pallas_call | solution.py:674
  102.6 2.3 %copy.12 = bf16[256,2048]{1,0:T(8,128)(2,1)} copy(bf16[256,2048]{1,0:T(8,128)(2,1)} %layer_all.1) | data formatting | bytes 2097152

commit v4 on v3

--- a/solution.py
+++ b/solution.py
@@ -13,8 +13,8 @@
 LANES = 128
 EPS = 1e-06
 MESH = pl.DeviceIdType.MESH
-KINDS = 14
-X, Y, DX, DY, XP, YP, FX, FY, FDX, FDY, GX, GY, GDX, GDY = range(KINDS)
+KINDS = 16
+X, Y, DX, DY, XP, YP, FX, FY, FDX, FDY, GX, GY, GDX, GDY, GXH, GYH = range(KINDS)
 
 def from_behind(value, axis, steps):
     count = lax.axis_size(axis)
@@ -134,8 +134,8 @@
         partner = self.z * CORES + (1 - self.c)
         self.partner = (partner, self.tp)
         along_x, along_y = (self.sp, self.tx), (self.sp, self.ty)
-        self.to = {kind: along_x for kind in (X, XP, DX, FX, FDX, GX, GDX)}
-        self.to.update({kind: along_y for kind in (Y, YP, DY, FY, FDY, GY, GDY)})
+        self.to = {kind: along_x for kind in (X, XP, DX, FX, FDX, GX, GDX, GXH)}
+        self.to.update({kind: along_y for kind in (Y, YP, DY, FY, FDY, GY, GDY, GYH)})
 
     def copy(self, kind, index, src, dst):
         return pltpu.make_async_remote_copy(
@@ -165,7 +165,7 @@
     hello(place.to[Y])
     for step in range(1, count):
         hello((lax.rem(place.sp + step, count), place.tp))
-    pl.semaphore_wait(barrier, count + 1)
+    return lambda: pl.semaphore_wait(barrier, count + 1)
 
 
 def level_order(place):
@@ -184,14 +184,16 @@
 
 
 PLAN = [
-    ("spread_line", 0), ("relay", 2), ("relay", 1), ("spread_diagonal", 0), ("spread_line", 1),
-    ("spread_last", 0), ("pick", 0), ("grow", 0), ("spread_line", 2), ("shrink", 0),
-    ("spread_diagonal", 1), ("relay", 3), ("relay_diagonal", 1), ("spread_last", 1), ("first", 0),
-    ("pick", 1), ("relay_diagonal", 2), ("grow", 1), ("shrink", 1), ("spread_line", 3),
-    ("spread_diagonal", 2), ("first", 1), ("spread_last", 2), ("relay_diagonal", 3), ("pick", 2),
-    ("grow", 2), ("shrink", 2), ("spread_diagonal", 3), ("spread_last", 3), ("first", 2),
-    ("pick", 3), ("grow", 3), ("shrink", 3), ("second", 2), ("first", 3), ("third", 2),
-    ("second", 3), ("third", 3), ("second", 1), ("second", 0), ("third", 1), ("finish", 0),
+    ("spread_line", 0), ("spread_diagonal", 0), ("relay", 2), ("relay", 1), ("relay_rest", 1),
+    ("relay_rest", 2), ("spread_line", 1), ("spread_last", 0), ("pick", 0), ("spread_line", 2),
+    ("relay", 3), ("grow", 0), ("shrink", 0), ("relay_rest", 3), ("relay_diagonal", 2),
+    ("first", 0), ("relay_diagonal_rest", 2), ("spread_diagonal", 2), ("relay_diagonal", 1),
+    ("spread_diagonal", 1), ("relay_diagonal_rest", 1), ("spread_last", 1), ("spread_line", 3),
+    ("pick", 1), ("grow", 1), ("relay_diagonal", 3), ("shrink", 1), ("relay_diagonal_rest", 3),
+    ("spread_last", 2), ("first", 1), ("pick", 2), ("grow", 2), ("shrink", 2), ("second", 1),
+    ("spread_diagonal", 3), ("spread_last", 3), ("first", 2), ("pick", 3), ("grow", 3),
+    ("shrink", 3), ("third", 1), ("second", 2), ("first", 3), ("third", 2), ("second", 3),
+    ("third", 3), ("second", 0), ("finish", 0),
 ]
 
 
@@ -201,7 +203,8 @@
     plan = []
     for turn in range(levels + 3):
         step = turn - 2
-        plan += [("relay", turn), ("relay_diagonal", step)]
+        plan += [("relay", turn), ("relay_rest", turn)]
+        plan += [("relay_diagonal", step), ("relay_diagonal_rest", step)]
         plan += [("spread_line", turn), ("spread_diagonal", turn - 1), ("spread_last", step)]
         plan += [("pick", step), ("first", step - 1), ("grow", step), ("second", step - 2)]
         plan += [("shrink", step), ("third", step - 3)]
@@ -256,33 +259,36 @@
     middle = (z > 0) & (z < place.levels - 1)
     has_up, has_down = z < place.levels - 1, z > 0
 
-    def line(level, diagonal, up=True):
-        ref = block(level, c, place.td if diagonal else tp)
+    def line(level, diagonal, part_of, up=True):
+        ref = block(level, c, place.td if diagonal else tp, part_of * half, half)
+        lane = 2 * diagonal + part_of
         return pltpu.make_async_remote_copy(
             src_ref=ref,
             dst_ref=ref,
-            send_sem=z_send.at[2 * diagonal + up, level],
-            recv_sem=z_recv.at[diagonal, level],
+            send_sem=z_send.at[2 * lane + up, level],
+            recv_sem=z_recv.at[lane, level],
             device_id=((z + 1 if up else z - 1) * CORES + c, tp),
             device_id_type=MESH,
         )
 
     def line_own(diagonal, act):
-        pl.when(has_up)(lambda: act(line(z, diagonal, True)))
-        pl.when(has_down)(lambda: act(line(z, diagonal, False)))
-
-    def line_on(level, diagonal, act):
-        pl.when(middle & (level < z))(lambda: act(line(level, diagonal, True)))
-        pl.when(middle & (level > z))(lambda: act(line(level, diagonal, False)))
-
-    def line_relay(step, diagonal):
+        for part_of in range(2):
+            pl.when(has_up)(lambda: act(line(z, diagonal, part_of, True)))
+            pl.when(has_down)(lambda: act(line(z, diagonal, part_of, False)))
+
+    def line_on(level, diagonal, part_of, act):
+        pl.when(middle & (level < z))(lambda: act(line(level, diagonal, part_of, True)))
+        pl.when(middle & (level > z))(lambda: act(line(level, diagonal, part_of, False)))
+
+    def line_relay(step, diagonal, part_of):
         level = order[step]
         if step:
-            pl.when(middle)(lambda: line(level, diagonal).wait_recv())
-            line_on(level, diagonal, lambda copy: copy.start())
+            pl.when(middle)(lambda: line(level, diagonal, part_of).wait_recv())
+            line_on(level, diagonal, part_of, lambda copy: copy.start())
 
     def line_end(level, diagonal):
-        pl.when(jnp.logical_not(middle))(lambda: line(level, diagonal).wait_recv())
+        for part_of in range(2):
+            pl.when(jnp.logical_not(middle))(lambda: line(level, diagonal, part_of).wait_recv())
 
     def core_copy(level, tile, core):
         ref = block(level, core, tile)
@@ -303,30 +309,44 @@
         ref = block(level, c, tile, 0 if kind == GDY else half, half)
         return place.copy(kind, level, ref, ref)
 
+    def own_half(kind, tile, part_of):
+        ref = block(z, c, tile, part_of * half, half)
+        return place.copy(kind, part_of, ref, ref)
+
     def spread_line(step):
         level = order[step]
         if step:
             line_end(level, 0)
-        whole(GX, level, tp).start()
-        whole(GY, level, tp).start()
+            whole(GX, level, tp).start()
+            whole(GY, level, tp).start()
+        else:
+            for part_of in range(2):
+                own_half(GXH, tp, part_of).start()
+                own_half(GYH, tp, 1 - part_of).start()
         core_copy(level, tp, c).start()
 
     def spread_diagonal(step):
         level = order[step]
-        whole(GX, level, place.tx).wait_recv()
-        if step == 0:
+        if step:
+            whole(GX, level, place.tx).wait_recv()
+            core_copy(level, place.tx, c).start()
+            whole(GY, level, place.ty).wait_recv()
+            core_copy(level, place.ty, c).start()
+        else:
+            own_half(GXH, place.tx, 0).wait_recv()
             part(GDY, level, place.tx).start()
-        core_copy(level, place.tx, c).start()
-        whole(GY, level, place.ty).wait_recv()
-        if step == 0:
+            own_half(GYH, place.ty, 1).wait_recv()
             part(GDX, level, place.ty).start()
-        core_copy(level, place.ty, c).start()
 
     def spread_last(step):
         level = order[step]
         if step:
             line_end(level, 1)
         else:
+            own_half(GXH, place.tx, 1).wait_recv()
+            core_copy(level, place.tx, c).start()
+            own_half(GYH, place.ty, 0).wait_recv()
+            core_copy(level, place.ty, c).start()
             part(GDY, level, place.td).wait_recv()
             part(GDX, level, place.td).wait_recv()
             line_own(1, lambda copy: copy.start())
@@ -446,8 +466,8 @@
         return pltpu.make_async_remote_copy(
             src_ref=s_z.at[level, at],
             dst_ref=r_z.at[level if arriving else z, at],
-            send_sem=z_send.at[4 + part_of, level],
-            recv_sem=z_recv.at[2 + part_of, level if arriving else z],
+            send_sem=z_send.at[8 + part_of, level],
+            recv_sem=z_recv.at[4 + part_of, level if arriving else z],
             device_id=(level * CORES + c, tp),
             device_id_type=MESH,
         )
@@ -563,16 +583,16 @@
         extended[SPAN:] = value.astype(jnp.float32)
         rim_out[...] = value[rows - SPAN :]
 
-    def mix():
-        extended[:SPAN] = rim_in[...].astype(jnp.float32)
-        value = extended[...]
+    def mix(begin, end):
+        value = extended[begin : SPAN + end]
         sums, reach = value, 1
         window_sum = jnp.zeros_like(value)
         for group in range(GROUPS):
             sums = sums + pltpu.roll(sums, reach, 0)
             reach = 2 * reach
             window_sum = jnp.where(tp == group, sums, window_sum)
-        position = place.sp * rows + lax.broadcasted_iota(jnp.int32, (rows, 1), 0)
+        count = end - begin
+        position = place.sp * rows + begin + lax.broadcasted_iota(jnp.int32, (count, 1), 0)
         window = 2
         for group in range(1, GROUPS):
             window = jnp.where(tp == group, 2 ** (group + 1), window)
@@ -580,10 +600,11 @@
         pooled = (window_sum[SPAN:] / divisor - value[SPAN:]).astype(jnp.bfloat16)
         mixed = jnp.dot(pooled, pool_ref[...], preferred_element_type=jnp.float32)
         mixed = (mixed * pool_scale_ref[...]).astype(jnp.bfloat16).astype(jnp.float32)
-        after = (stream_ref[:, mine].astype(jnp.float32) + mixed).astype(jnp.bfloat16)
-        own_ref[...] = after
-        held[z, pl.ds(pl.multiple_of(c * rows, rows), rows), mine] = after
-
+        after = (stream_ref[begin:end, mine].astype(jnp.float32) + mixed).astype(jnp.bfloat16)
+        own_ref[begin:end] = after
+        held[z, pl.ds(pl.multiple_of(c * rows + begin, SPAN), count), mine] = after
+
+    greeted = greet(place)
     for piece in range(pieces):
         gate_copy(piece, 0).start()
         gate_copy(piece, 1).start()
@@ -596,17 +617,21 @@
     local_meta.start()
     pl.when(place.sp == 0)(lambda: rim_in.__setitem__(Ellipsis, jnp.zeros_like(rim_in)))
     local_meta.wait()
-    greet(place)
+    greeted()
     pl.when(place.sp < sp_count - 1)(lambda: rim_copy(1).start())
     for hop in range(1, sp_count):
         meta_copy(hop).start()
+    mix(SPAN, rows)
     pl.when(place.sp > 0)(lambda: rim_copy(-1).wait_recv())
-    mix()
+    extended[:SPAN] = rim_in[...].astype(jnp.float32)
+    mix(0, SPAN)
     line_own(0, lambda copy: copy.start())
 
     stages = {
-        "relay": lambda step: line_relay(step, 0),
-        "relay_diagonal": lambda step: line_relay(step, 1),
+        "relay": lambda step: line_relay(step, 0, 0),
+        "relay_rest": lambda step: line_relay(step, 0, 1),
+        "relay_diagonal": lambda step: line_relay(step, 1, 0),
+        "relay_diagonal_rest": lambda step: line_relay(step, 1, 1),
         "spread_line": spread_line,
         "spread_diagonal": spread_diagonal,
         "spread_last": spread_last,
@@ -633,8 +658,6 @@
     line_own(0, lambda copy: copy.wait_send())
     line_own(1, lambda copy: copy.wait_send())
     for step, level in enumerate(order):
-        whole(GX, level, tp).wait_send()
-        whole(GY, level, tp).wait_send()
         for tile in range(tiles):
             core_copy(level, tile, c).wait_send()
             pair_copy(level, tile).wait_send()
@@ -644,9 +667,15 @@
             side(kind, level).wait_send()
         if step:
             for part_of in range(2):
-                line_on(level, part_of, lambda copy: copy.wait_send())
+                line_on(level, 0, part_of, lambda copy: copy.wait_send())
+                line_on(level, 1, part_of, lambda copy: copy.wait_send())
                 owner_copy(level, part_of, False).wait_send()
+            whole(GX, level, tp).wait_send()
+            whole(GY, level, tp).wait_send()
         else:
+            for part_of in range(2):
+                own_half(GXH, tp, part_of).wait_send()
+                own_half(GYH, tp, part_of).wait_send()
             part(GDY, level, place.tx).wait_send()
             part(GDX, level, place.ty).wait_send()
     final(FDY, place.td, 0).wait_recv()
@@ -701,8 +730,8 @@
             pltpu.SemaphoreType.DMA((levels, tp_count)),
             pltpu.SemaphoreType.DMA((levels, tp_count)),
             pltpu.SemaphoreType.DMA((levels, tp_count)),
+            pltpu.SemaphoreType.DMA((10, levels)),
             pltpu.SemaphoreType.DMA((6, levels)),
-            pltpu.SemaphoreType.DMA((4, levels)),
             pltpu.SemaphoreType.DMA((sp_count,)),
             pltpu.SemaphoreType.DMA((sp_count,)),
             pltpu.SemaphoreType.DMA((pieces + 1, 2)),

time: 105 us -> 97.8 us (0.931)
  Pallas kernels: 103 us -> 95.3 us
    pallas_call x1, Pallas kernels: 103 us -> 95.3 us  [layer_all(): pl.pallas_call(layer_kernel, out_shape=jax.ShapeDtypeStruct((rows, width)...]
where the time goes in v4:
time: 97.8 us; the launch traced here: 97.6 us
  Pallas kernels  95.3 us (97%)
  local copies, waits for them, and re-layouts  2.3 us (2%)
    pallas_call x1, Pallas kernels, layer_all(): pl.pallas_call(layer_kernel, out_shape=jax.ShapeDtypeStruct((rows, width)...  95.3 us
    unnamed x1, local copies, waits for them, and re-layouts  2.3 us

profile of v4, /device:TPU:0, one launch (start us, length us, event | category | flops | bytes accessed | tf_op | source)
XLA Modules:
  0.0 97.6 jit_solution(9024630827745580906)
XLA Ops:
  0.0 95.3 %layer_all.1 = bf16[256,2048]{1,0:T(8,128)(2,1)} custom-call(bf16[256,2048]{1,0:T(8,128)(2,1)} %stream_ref.1, f32[1,2048]{1,0:T(1,128)} %bitcast.5, bf16[512,512]{1,0:T(8,128)(2,1)} %pool_ref.1, f32[1,512]{1,0:T(1,128)} %bitcast.7, s32[2,256]{1,0:T(2,128)} %bitcast.8, f32[2,256]{1,0:T(2,128)} %bitcast.9, f32[1,2048]{1,0:T(1,128)} %bitcast.6, ...), custom_call_target="tpu_custom_call" | custom-call | tf_op jit(solution)/shard_map/layer_all/pallas_call | solution.py:703
  95.3 2.3 %copy.12 = bf16[256,2048]{1,0:T(8,128)(2,1)} copy(bf16[256,2048]{1,0:T(8,128)(2,1)} %layer_all.1) | data formatting | bytes 2097152
